TPU v7x, 32 devices: a whole 2x2x4 slice. The times are simulated.
32 devices in a mesh: sp: 8 (over z, x), tp: 4 (over y, core).
Axes of the slice: x: 2, y: 2, z: 4, core: 2. Of those that a mesh axis runs over, the one named last changes fastest.
Arguments:
- readout_query_vectors: bfloat16 [2048, 2048], P('sp', 'tp'), may hold values from -6 to 6
- attention_key_vectors: bfloat16 [2048, 2048], P('sp', 'tp'), may hold values from -6 to 6
- attention_content_vectors: bfloat16 [2048, 2048], P('sp', 'tp'), may hold values from -6 to 6
- step_size_preactivation: bfloat16 [2048, 2048], P('sp', 'tp'), may hold values from -16 to 8
- forgetting_preactivation: float32 [2048, 2048], P('sp', 'tp'), may hold values from -22 to 3
- extra_forgetting_bias: float32 [2048, 32], P('sp', 'tp'), may hold values from -0.7 to 0
- subspace_normalizer_gain: float32 [2048], P('tp'), may hold values from 0.1 to 1.9
- skip_connection_stream: bfloat16 [2048, 2048], P('sp'), may hold values from -40 to 40
- blender_projection_matrix: bfloat16 [2048, 2048], P('tp'), may hold values from -0.125 to 0.125
- specialist_prenormal_gain: float32 [2048], replicated, may hold values from 0.1 to 1.9
- cluster_router_chance: float32 [2048], P('sp'), may hold values from 0.4 to 1
- specialist_chance_within_cluster: float32 [2048, 2], P('sp'), may hold values from 0.1 to 1
- chosen_specialist_ids: int32 [2048, 2], P('sp'), may hold values from 0 to 7, all different within a row; in each aligned block of 256 rows (0 to 255, 256 to 511, ...) at most 128 rows name the same one
- specialist_switch_matrix: bfloat16 [8, 2048, 2048], P('sp', None, 'tp'), may hold values from -0.125 to 0.125
- specialist_expansion_matrix: bfloat16 [8, 2048, 2048], P('sp', None, 'tp'), may hold values from -0.125 to 0.125
- specialist_contraction_matrix: bfloat16 [8, 2048, 2048], P('sp', 'tp'), may hold values from -0.375 to 0.375
Outputs:
- layer_out: bfloat16 [2048, 2048], P('sp')
Inputs may be any that keep to these rules, and one draw needn't show every extreme that they name: `chosen_specialist_ids`: in each aligned block of 256 rows every expert is named at most 128 times.
All inputs are finite; a program needn't handle non-finite values.
Results may differ from a plain program's by a relative error of at most 0.022.
Values may be sent and summed in bfloat16 or wider, within the bound.
A program may use at most 64 MiB of HBM per device.

v0:
```python
import jax
import jax.numpy as jnp
from jax import lax
from jax.sharding import PartitionSpec as P

HIGH = lax.Precision.HIGHEST


def carried_in(shard, axis, combine, identity):
    count, position = (lax.axis_size(axis), lax.axis_index(axis))
    everything = jax.tree.map(
        lambda part, kind: lax.all_gather(part.astype(kind), axis),
        shard,
        (jnp.bfloat16, jnp.bfloat16),
    )
    start = jax.tree.map(
        lambda part, zero: jnp.broadcast_to(jnp.asarray(zero, part.dtype), part.shape),
        shard,
        identity,
    )

    def hop(k, before):
        reached = k < position
        new = combine(
            before, jax.tree.map(lambda part, own: part[k].astype(own.dtype), everything, shard)
        )
        return jax.tree.map(lambda a, b: jnp.where(reached, a, b), new, before)

    return lax.fori_loop(0, count, hop, start)


def compose(earlier, following):
    keep_first, add_first = earlier
    keep_second, add_second = following
    return (
        jnp.matmul(keep_first, keep_second, precision=HIGH),
        jnp.matmul(add_first, keep_second, precision=HIGH) + add_second,
    )


def inner_pairs(left, right):
    return jnp.einsum("bhsd,bhtd->bhst", left, right, precision=HIGH)


def times_rows(matrix, data):
    return jnp.einsum("bhst,bhtd->bhsd", matrix, data, precision=HIGH)


def token_mixer_layer(
    readout_query_vectors,
    attention_key_vectors,
    attention_content_vectors,
    step_size_preactivation,
    forgetting_preactivation,
    extra_forgetting_bias,
    subspace_normalizer_gain,
):
    segment = 64
    tok_rows = readout_query_vectors.shape[0]
    attention_subspace_count = extra_forgetting_bias.shape[1]
    blocks = tok_rows // segment

    def reorder_sharding(data):
        return (
            data.astype(jnp.float32)
            .reshape(blocks, segment, attention_subspace_count, -1)
            .transpose(0, 2, 1, 3)
        )

    query_rows = reorder_sharding(readout_query_vectors)
    key_rows = reorder_sharding(attention_key_vectors)
    value_rows = reorder_sharding(attention_content_vectors)
    learn_rate = jax.nn.sigmoid(reorder_sharding(step_size_preactivation))
    logarithmic_forgetting_amounts = reorder_sharding(
        -jnp.exp(-jax.nn.softplus(-forgetting_preactivation) - 0.5)
    ) + reorder_sharding(extra_forgetting_bias)
    head_dim = key_rows.shape[-1]
    removal = key_rows / jnp.sqrt(jnp.sum(key_rows * key_rows, axis=-1, keepdims=True) + 1e-06)
    cumulative = jnp.cumsum(logarithmic_forgetting_amounts, axis=2)
    closing = cumulative[:, :, -1:, :]
    alpha_tilde = -removal * jnp.exp(cumulative - logarithmic_forgetting_amounts)
    beta_rows = removal * learn_rate
    beta_hat = beta_rows * jnp.exp(-cumulative)
    key_hat = key_rows * jnp.exp(-cumulative)
    query_tilde = query_rows * jnp.exp(cumulative)
    beta_bar = beta_rows * jnp.exp(closing - cumulative)
    key_bar = key_rows * jnp.exp(closing - cumulative)
    offsets = jnp.arange(segment)
    strict = (offsets[:, None] > offsets[None, :]).astype(jnp.float32)
    inclusive = (offsets[:, None] >= offsets[None, :]).astype(jnp.float32)
    remove_remove = inner_pairs(alpha_tilde, beta_hat) * strict
    remove_write = inner_pairs(alpha_tilde, key_hat) * strict
    read_remove = inner_pairs(query_tilde, beta_hat) * inclusive
    read_write = inner_pairs(query_tilde, key_hat) * inclusive
    system = jnp.eye(segment, dtype=jnp.float32) - remove_remove
    right_side = jnp.concatenate([alpha_tilde, times_rows(remove_write, value_rows)], axis=-1)
    solved = jax.scipy.linalg.solve_triangular(system, right_side, lower=True, unit_diagonal=True)
    absorb = solved[..., :head_dim]
    carried_rows = solved[..., head_dim:]
    key_eye = jnp.eye(head_dim, dtype=jnp.float32)
    keep_block = jnp.einsum(
        "bhsk,bhsj->bhkj", absorb, beta_bar, precision=HIGH
    ) + key_eye * jnp.exp(closing)
    add_block = jnp.einsum("bhsv,bhsk->bhvk", carried_rows, beta_bar, precision=HIGH) + jnp.einsum(
        "bhsv,bhsk->bhvk", value_rows, key_bar, precision=HIGH
    )
    local_out = times_rows(read_remove, carried_rows) + times_rows(read_write, value_rows)
    readout_map = query_tilde + times_rows(read_remove, absorb)
    keep_prefix, add_prefix = lax.associative_scan(compose, (keep_block, add_block), axis=0)
    zero_state = jnp.zeros((attention_subspace_count, head_dim, head_dim), jnp.float32)
    identity = (jnp.broadcast_to(key_eye, zero_state.shape), zero_state)
    incoming = carried_in((keep_prefix[-1], add_prefix[-1]), "sp", compose, identity)[1]
    keep_before = jnp.concatenate([identity[0][None], keep_prefix[:-1]], axis=0)
    add_before = jnp.concatenate([zero_state[None], add_prefix[:-1]], axis=0)
    starts = jnp.matmul(incoming[None], keep_before, precision=HIGH) + add_before
    output = local_out + jnp.einsum("bhsk,bhvk->bhsv", readout_map, starts, precision=HIGH)
    centered = output - jnp.mean(output, axis=-1, keepdims=True)
    spread = jnp.mean(centered * centered, axis=-1, keepdims=True)
    gains = subspace_normalizer_gain.reshape(attention_subspace_count, head_dim)[None, :, None, :]
    normed = centered * lax.rsqrt(spread + 0.00064) * gains
    return (
        normed.transpose(0, 2, 1, 3)
        .reshape(tok_rows, attention_subspace_count * head_dim)
        .astype(jnp.bfloat16)
    )


def body(
    readout_query_vectors,
    attention_key_vectors,
    attention_content_vectors,
    step_size_preactivation,
    forgetting_preactivation,
    extra_forgetting_bias,
    subspace_normalizer_gain,
    skip_connection_stream,
    blender_projection_matrix,
    specialist_prenormal_gain,
    cluster_router_chance,
    specialist_chance_within_cluster,
    chosen_specialist_ids,
    specialist_switch_matrix,
    specialist_expansion_matrix,
    specialist_contraction_matrix,
):
    blender_result = token_mixer_layer(
        readout_query_vectors,
        attention_key_vectors,
        attention_content_vectors,
        step_size_preactivation,
        forgetting_preactivation,
        extra_forgetting_bias,
        subspace_normalizer_gain,
    )
    branch = lax.psum(
        jnp.dot(
            blender_result, blender_projection_matrix, preferred_element_type=jnp.float32
        ).astype(jnp.bfloat16),
        "tp",
    ).astype(jnp.float32)
    hidden_state = skip_connection_stream.astype(jnp.float32) + branch
    inverse_rms = lax.rsqrt(jnp.mean(hidden_state * hidden_state, axis=1, keepdims=True) + 1e-06)
    normed = (hidden_state * inverse_rms * specialist_prenormal_gain).astype(jnp.bfloat16)
    tok_rows = skip_connection_stream.shape[0]
    model_width = skip_connection_stream.shape[1]
    local_experts = specialist_switch_matrix.shape[0]
    experts = local_experts * lax.axis_size("sp")
    top_count = chosen_specialist_ids.shape[1]
    capacity = 2 * tok_rows * top_count // experts
    flat_expert = chosen_specialist_ids.reshape(-1)
    one_hot = (flat_expert[:, None] == jnp.arange(experts, dtype=jnp.int32)[None, :]).astype(
        jnp.int32
    )
    earlier = jnp.sum((jnp.cumsum(one_hot, axis=0) - one_hot) * one_hot, axis=1)
    slot_index = flat_expert * capacity + earlier
    token_of = jnp.arange(flat_expert.shape[0], dtype=jnp.int32) // top_count
    slot_owner = jnp.full((experts * capacity,), tok_rows, jnp.int32).at[slot_index].set(token_of)
    padded = jnp.concatenate([normed, jnp.zeros((1, model_width), jnp.bfloat16)], axis=0)
    outgoing = padded[slot_owner].reshape(experts, capacity, model_width)
    route_weight = (
        cluster_router_chance[:, None]
        * specialist_chance_within_cluster
        / jnp.sum(specialist_chance_within_cluster, axis=1, keepdims=True)
    )
    rows_in = lax.all_to_all(outgoing, "sp", split_axis=0, concat_axis=0, tiled=True)
    grouped = rows_in.reshape(-1, local_experts, rows_in.shape[1], model_width)
    gate_act = jnp.einsum(
        "secd,edf->secf", grouped, specialist_switch_matrix, preferred_element_type=jnp.float32
    )
    upward = jnp.einsum(
        "secd,edf->secf", grouped, specialist_expansion_matrix, preferred_element_type=jnp.float32
    )
    hidden = (jax.nn.silu(gate_act) * upward).astype(jnp.bfloat16)
    partial_value = jnp.einsum(
        "secf,efd->secd", hidden, specialist_contraction_matrix, preferred_element_type=jnp.float32
    )
    partial_value = partial_value.astype(jnp.bfloat16).reshape(rows_in.shape)
    summed = lax.psum_scatter(
        partial_value.astype(jnp.float32).astype(jnp.bfloat16),
        "tp",
        scatter_dimension=2,
        tiled=True,
    ).astype(jnp.float32)
    returned = lax.all_to_all(
        summed.astype(jnp.bfloat16), "sp", split_axis=0, concat_axis=0, tiled=True
    ).astype(summed.dtype)
    column_count = returned.shape[2]
    picked = returned.reshape(experts * capacity, column_count)[slot_index].reshape(
        tok_rows, top_count, column_count
    )
    mixture = jnp.sum(route_weight[:, :, None] * picked, axis=1)
    own_columns = lax.dynamic_slice_in_dim(
        hidden_state, lax.axis_index("tp") * column_count, column_count, 1
    )
    return lax.all_gather((own_columns + mixture).astype(jnp.bfloat16), "tp", axis=1, tiled=True)


def solution(mesh):
    in_specs = (
        P("sp", "tp"),
        P("sp", "tp"),
        P("sp", "tp"),
        P("sp", "tp"),
        P("sp", "tp"),
        P("sp", "tp"),
        P("tp"),
        P("sp", None),
        P("tp", None),
        P(),
        P("sp"),
        P("sp", None),
        P("sp", None),
        P("sp", None, "tp"),
        P("sp", None, "tp"),
        P("sp", "tp", None),
    )
    out_specs = P("sp", None)
    return jax.shard_map(body, mesh=mesh, in_specs=in_specs, out_specs=out_specs, check_vma=False)
```

profile of v0, /device:TPU:0, one launch (start us, length us, event | category | flops | bytes accessed | tf_op | source)
XLA Modules:
  0.0 655.8 jit_solution(5409190180976845253)
XLA Ops:
  6.6 2.4 fusion.58
  8.9 1.2 reshape.178
  12.3 1.2 reshape.197
  13.5 1.6 fusion.41
  15.1 1.9 add_divide_fusion
  17.0 2.2 reshape.193
  19.3 3.6 fusion.50
  22.9 3.1 convolution_multiply_fusion.1
  26.0 2.8 fusion.26
  28.8 158.8 %custom-call.4 = f32[4,8,1,64,64]{3,4,2,1,0:T(8,128)} custom-call(f32[4,8,1,64,64]{4,3,2,1,0:T(8,128)} %fusion.26), custom_call_target="InvertDiagBlocksLowerTriangular" | custom-call | tf_op jit(solution)/shard_map/jit(_solve_triangular)/vmap(vmap())/triangular_solve | solution.py:97
  187.6 2.1 reshape.181
  189.7 2.5 convolution_bitcast_fusion.2
  193.8 2.1 fusion.30
  196.0 2.2 convolution_add_fusion.1
  198.2 1.9 convolution_add_fusion.2
  202.7 1.1 fusion.29
  206.9 1.9 pad_maximum_fusion.1
  208.9 9.2 %pad.34 = f32[4,8,64,64]{3,2,1,0:T(8,128)} pad(f32[2,8,64,64]{3,2,1,0:T(8,128)} %pad_maximum_fusion.1, f32[]{:T(128)} %constant.82.clone.1), padding=0_1_1x0_0_0x0_0_0x0_0_0 | pad | bytes 786436 | tf_op jit(solution)/shard_map/pad | solution.py:109
  218.0 9.1 %pad.50 = f32[3,8,64,64]{3,2,1,0:T(8,128)} pad(f32[2,8,64,64]{3,2,1,0:T(8,128)} %pad_maximum_fusion.1, f32[]{:T(128)} %constant.82.clone.1), padding=0_0_1x0_0_0x0_0_0x0_0_0 | pad | bytes 655364 | tf_op jit(solution)/shard_map/slice | solution.py:114
  227.1 1.8 pad_maximum_fusion
  228.9 9.2 %pad.30 = f32[4,8,64,64]{3,2,1,0:T(8,128)} pad(f32[2,8,64,64]{3,2,1,0:T(8,128)} %pad_maximum_fusion, f32[]{:T(128)} %constant.82.clone.1), padding=0_1_1x0_0_0x0_0_0x0_0_0 | pad | bytes 786436 | tf_op jit(solution)/shard_map/pad | solution.py:109
  238.1 9.3 %pad.48 = f32[3,8,64,64]{3,2,1,0:T(8,128)} pad(f32[2,8,64,64]{3,2,1,0:T(8,128)} %pad_maximum_fusion, f32[]{:T(128)} %constant.82.clone.1), padding=0_0_1x0_0_0x0_0_0x0_0_0 | pad | bytes 655364 | tf_op jit(solution)/shard_map/slice | solution.py:113
  247.4 2.1 reshape.196
  249.5 3.8 convolution_multiply_fusion.3
  253.3 2.5 convolution_add_fusion.3
  255.8 3.1 fusion.47
  258.9 3.3 convolution_multiply_fusion
  262.3 6.2 pad.98
  270.4 36.7 %all_gather.12 = bf16[8,8,64,64]{3,2,1,0:T(8,128)(2,1)} all-gather(bf16[1,8,64,64]{3,2,1,0:T(8,128)(2,1)S(1)} %add_convert_fusion.1), channel_id=1, replica_groups=mesh['sp'=8,'tp'=4] {'sp'}, dimensions={0}, use_global_device_ids=true | all-gather | bytes 589824 | tf_op jit(solution)/shard_map/all_gather | solution.py:12
  307.1 9.2 %pad.97 = f32[4,8,64,64]{3,2,1,0:T(8,128)} pad(f32[2,8,64,64]{3,2,1,0:T(8,128)} %pad_add_fusion.1, f32[]{:T(128)} %constant.82.clone.1), padding=1_0_1x0_0_0x0_0_0x0_0_0 | pad | bytes 786436
  317.4 35.0 %all_gather.11 = bf16[8,8,64,64]{3,2,1,0:T(8,128)(2,1)} all-gather(bf16[1,8,64,64]{3,2,1,0:T(8,128)(2,1)S(1)} %add_convert_fusion.2), channel_id=1, replica_groups=mesh['sp'=8,'tp'=4] {'sp'}, dimensions={0}, use_global_device_ids=true | all-gather | bytes 589824 | tf_op jit(solution)/shard_map/all_gather | solution.py:12
  352.4 19.0 %while.14 = (s32[]{:T(128)}, f32[8,64,64]{1,2,0:T(8,128)S(1)}, s32[]{:T(128)}, bf16[8,8,64,64]{3,2,1,0:T(8,128)(2,1)}, bf16[8,8,64,64]{3,2,1,0:T(8,128)(2,1)}, /*index=5*/s32[]{:T(128)}, s32[]{:T(128)}) while((s32[]{:T(128)}, f32[8,64,64]{1,2,0:T(8,128)S(1)}, s32[]{:T(128)}, bf16[8,8,64,64]{3,2,1,0:T(8,128)(2,1)}, ...), condition=%wide.region_3.4_spmd.clone, body=%wide.region_2.3_spmd.clone.sunk | while | flops 25329668 | bytes 1443939 | solution.py:29
  353.8 1.2 fusion.123
  356.2 1.2 fusion.123
  358.5 1.2 fusion.123
  360.8 1.2 fusion.123
  363.2 1.2 fusion.123
  365.5 1.2 fusion.123
  367.8 1.2 fusion.123
  370.2 1.2 fusion.123
  371.5 1.4 slice_add_fusion
  372.8 1.5 slice_add_fusion.1
  376.6 1.8 fusion.101
  379.8 1.4 copy.110
  381.5 3.4 convolution_convert_fusion.1
  385.4 1.1 reduce-window.6
  387.2 2.4 scatter_custom_fusion
  389.7 32.5 %all-reduce.12.cloned.1.call-done = bf16[256,2048]{1,0:T(8,128)(2,1)} async-done(((bf16[256,2048]{1,0:T(8,128)(2,1)}), bf16[256,2048]{1,0:T(8,128)(2,1)}) %all-reduce.12.cloned.1.call-update) | async-done | bytes 1048592 | tf_op jit(solution)/shard_map/psum | solution.py:155
  422.2 3.0 convert_add_fusion
  425.8 6.0 gather_fusion
  431.8 98.6 %all_to_all.10 = bf16[8,128,2048]{2,1,0:T(8,128)(2,1)S(1)} all-to-all(bf16[8,128,2048]{2,1,0:T(8,128)(2,1)} %bitcast.213), channel_id=1, replica_groups=mesh['sp'=8,'tp'=4] {'sp'}, dimensions={0} | all-to-all | bytes 8388608 | tf_op jit(solution)/shard_map/all_to_all | solution.py:185
  530.4 2.0 copy-done.19
  532.4 3.7 fusion.11
  536.1 10.1 %convolution_convert_fusion = bf16[8,128,2048]{2,1,0:T(8,128)(2,1)} fusion(bf16[1,512,2048]{2,1,0:T(8,128)(2,1)S(1)} %copy-done, f32[8,128,512]{2,1,0:T(8,128)} %fusion.11, bf16[8,128,2048]{2,1,0:T(8,128)(2,1)} %copy-done.19, bf16[1,2048,512]{2,1,0:T(8,128)(2,1)} %param.31), kind=kOutput, calls=%fused_computation.14 | convolution fusion | flops 4300210176 | bytes 14680064 | tf_op jit(solution)/shard_map/secf,efd->secd/dot_general | solution.py:194
  546.2 43.2 %reduce-scatter.2.cloned.1.call-done = bf16[8,128,512]{2,1,0:T(8,128)(2,1)} async-done(((bf16[8,128,2048]{2,1,0:T(8,128)(2,1)}), bf16[8,128,512]{2,1,0:T(8,128)(2,1)}) %reduce-scatter.2.cloned.1.call-update) | async-done | bytes 1048592 | tf_op jit(solution)/shard_map/reduce_scatter | solution.py:198
  589.4 5.5 all-to-all-start.1
  595.2 25.4 %all-to-all-done.1 = bf16[8,128,512]{2,1,0:T(8,128)(2,1)S(1)} async-done(((bf16[8,128,512]{2,1,0:T(8,128)(2,1)}), bf16[8,128,512]{2,1,0:T(8,128)(2,1)S(1)}, u32[]{:S(2)}, u32[]{:S(2)}) %all-to-all-start.1) | async-done | bytes 1048608 | tf_op jit(solution)/shard_map/all_to_all | solution.py:204
  620.6 1.7 bitcast_convert_fusion
  622.3 3.6 gather_fusion.1
  625.9 1.6 reshape.190
  627.5 2.6 multiply_reduce_fusion.1
  630.1 1.8 add_convert_fusion
  631.9 14.9 %all-gather.2.cloned.1.call-done = bf16[256,2048]{1,0:T(8,128)(2,1)} async-done(((bf16[256,512]{1,0:T(8,128)(2,1)}), bf16[256,2048]{1,0:T(8,128)(2,1)}) %all-gather.2.cloned.1.call-update) | async-done | bytes 1048592 | tf_op jit(solution)/shard_map/all_gather | solution.py:215
  646.8 2.3 copy.198
  (151 shorter events, 26.8 us)
Async XLA Ops:
  6.5 529.5 %copy-start = (bf16[1,512,2048]{2,1,0:T(8,128)(2,1)S(1)}, bf16[1,512,2048]{2,1,0:T(8,128)(2,1)}, u32[]{:S(2)}) copy-start(bf16[1,512,2048]{2,1,0:T(8,128)(2,1)} %param.33) | copy-start | bytes 6291460
  6.5 3.6 copy-start.28
  6.5 415.6 %all-reduce.12.cloned.1.call-start = ((), (), s32[]{:S(2)}) async-start(), calls=%async_computation.3 | async-start | bytes 2097152 | tf_op jit(solution)/shard_map/psum | solution.py:155
  10.2 1.0 copy-start.11
  11.2 1.1 copy-start.25
  19.3 3.6 copy-start.1
  22.9 3.1 copy-start.6
  22.9 3.1 copy-start.9
  189.7 2.5 copy-start.13
  189.7 2.6 copy-start.22
  192.3 1.2 copy-start.7
  192.3 1.5 copy-start.24
  193.8 2.1 copy-start.10
  195.9 2.3 copy-start.3
  200.1 6.8 %copy-start.8 = (f32[4,8,64,64]{3,2,1,0:T(8,128)}, f32[4,8,64,64]{3,2,1,0:T(8,128)S(1)}, u32[]{:S(2)}) copy-start(f32[4,8,64,64]{3,2,1,0:T(8,128)S(1)} %convolution_add_fusion.2) | copy-start | bytes 1572868
  206.9 20.2 %slice-start = ((f32[4,8,64,64]{3,2,1,0:T(8,128)}), f32[1,8,64,64]{3,2,1,0:T(8,128)S(1)}, s32[]{:S(2)}) async-start(f32[4,8,64,64]{3,2,1,0:T(8,128)} %copy-done.8), calls=%async_computation.6 | async-start | bytes 524288 | tf_op jit(solution)/shard_map/slice | solution.py:109
  249.5 3.8 copy-start.4
  249.5 3.8 copy-start.5
  255.8 3.1 copy-start.2
  268.5 1.0 copy-start.21
  270.4 81.9 %copy-start.12 = (f32[8,64,64]{1,2,0:T(8,128)S(1)}, f32[8,64,64]{1,2,0:T(8,128)}, u32[]{:S(2)}) copy-start(f32[8,64,64]{1,2,0:T(8,128)} %custom-call.5) | copy-start | bytes 393220
  352.4 19.1 %copy-start.23 = (f32[3,8,64,64]{3,2,1,0:T(8,128)S(1)}, f32[3,8,64,64]{3,2,1,0:T(8,128)}, u32[]{:S(2)}) copy-start(f32[3,8,64,64]{3,2,1,0:T(8,128)} %pad.50) | copy-start | bytes 1179652
  371.4 2.9 copy-start.14
  371.4 2.9 copy-start.15
  371.4 2.9 copy-start.16
  375.4 1.2 copy-start.20
  376.6 2.0 copy-start.30
  381.5 3.5 copy-start.27
  381.5 40.7 %copy-start.17 = (bf16[256,2048]{1,0:T(8,128)(2,1)S(1)}, bf16[256,2048]{1,0:T(8,128)(2,1)}, u32[]{:S(2)}) copy-start(bf16[256,2048]{1,0:T(8,128)(2,1)} %param.25) | copy-start | bytes 3145732
  384.9 204.5 %reduce-scatter.2.cloned.1.call-start = ((), (), s32[]{:S(2)}) async-start(), calls=%async_computation.4 | async-start | bytes 5242880 | tf_op jit(solution)/shard_map/reduce_scatter | solution.py:198
  389.7 35.5 %copy-start.26 = (f32[2048]{0:T(1024)S(1)}, f32[2048]{0:T(1024)}, u32[]{:S(2)}) copy-start(f32[2048]{0:T(1024)} %param.27) | copy-start | bytes 24580
  422.2 3.0 copy-start.18
  431.8 100.6 %copy-start.32 = (bf16[1,2048,512]{2,1,0:T(8,128)(2,1)S(1)}, bf16[1,2048,512]{2,1,0:T(8,128)(2,1)}, u32[]{:S(2)}) copy-start(bf16[1,2048,512]{2,1,0:T(8,128)(2,1)} %param.32) | copy-start | bytes 6291460
  530.4 2.0 copy-start.19
  546.2 48.8 %copy-start.29 = (f32[256,2]{0,1:T(2,128)S(1)}, f32[256,2]{0,1:T(2,128)}, u32[]{:S(2)}) copy-start(f32[256,2]{0,1:T(2,128)} %param.29) | copy-start | bytes 6148
  546.2 48.8 %copy-start.31 = (f32[256]{0:T(256)S(1)}, f32[256]{0:T(256)}, u32[]{:S(2)}) copy-start(f32[256]{0:T(256)} %param.28) | copy-start | bytes 3076
  589.4 31.2 %all-to-all-start.1 = ((bf16[8,128,512]{2,1,0:T(8,128)(2,1)}), bf16[8,128,512]{2,1,0:T(8,128)(2,1)S(1)}, u32[]{:S(2)}, u32[]{:S(2)}) async-start(bf16[8,128,512]{2,1,0:T(8,128)(2,1)} %reduce-scatter.2.cloned.1.call-done), calls=%async_computation.2 | async-start | bytes 2097152 | tf_op jit(solution)/shard_map/all_to_all | solution.py:204
  594.9 51.9 %all-gather.2.cloned.1.call-start = ((), (), s32[]{:S(2)}) async-start(), calls=%async_computation.5 | async-start | bytes 1310720 | tf_op jit(solution)/shard_map/all_gather | solution.py:215
Sparse Core Ops, SparseCore 0:
  385.0 37.0 all-reduce.11
  546.3 43.1 reduce-scatter.1
  632.1 14.7 all-gather.1
where the time goes:
time: 668 us; the launch traced here: 656 us
  other arithmetic  192 us (29%)
  blocking collectives  170 us (25%)
  waiting for transfers between devices  116 us (17%)
  local copies, waits for them, and re-layouts  94.1 us (14%)
  matrix products  63.1 us (9%)
  between operations  14 us (2%)
    another operation x3, other arithmetic, token_mixer_layer(): jax.scipy.linalg.solve_triangular(system, right_side, lower=True, unit_di...  159 us
    all_to_all x1, blocking collectives, body(): lax.all_to_all(outgoing, 'sp', split_axis=0, concat_axis=0, tiled=True)  98.6 us
    all_gather x2, blocking collectives, carried_in(): lax.all_gather(part.astype(kind), axis)  71.7 us
    reduce_scatter x1, waiting for transfers between devices, body(): lax.psum_scatter(partial_value.astype(jnp.float32).astype(jnp.bfloat16),...  43.2 us
    psum x1, waiting for transfers between devices, body(): lax.psum(jnp.dot(blender_result, blender_projection_matrix, preferred_ele...  32.5 us
    all_to_all x1, waiting for transfers between devices, body(): lax.all_to_all(summed.astype(jnp.bfloat16), 'sp', split_axis=0, concat_ax...  25.4 us
    unnamed x70, local copies, waits for them, and re-layouts  22.7 us
    pad x2, local copies, waits for them, and re-layouts, token_mixer_layer(): lax.associative_scan(compose, (keep_block, add_block), axis=0)  18.4 us
  transfers between devices with their start and end apart: 4, of which 4 were waited for; matrix products, arithmetic and copies ran while one was open for 1% of the time, Pallas kernels for 0%

commit v1 on v0

v1 whole, which is shorter than its diff:
```python
import functools

import jax
import jax.numpy as jnp
from jax import lax
from jax.experimental import pallas as pl
from jax.experimental.pallas import tpu as pltpu
from jax.sharding import PartitionSpec as P

MESH = pl.DeviceIdType.MESH
F32 = jnp.float32
BF16 = jnp.bfloat16


def dot(left, right, axes=(1, 0)):
    return lax.dot_general(
        left, right, (((axes[0],), (axes[1],)), ((), ())), preferred_element_type=F32
    )


def halves(data):
    high = data.astype(BF16)
    return high, (data - high.astype(F32)).astype(BF16)


def dot3(left, right, axes=(1, 0)):
    lh, ll = halves(left)
    rh, rl = halves(right)
    return dot(lh, rh, axes) + (dot(lh, rl, axes) + dot(ll, rh, axes))


def dot1(left, right, axes=(1, 0)):
    return dot(left.astype(BF16), right.astype(BF16), axes)


def mixer_kernel(head_dim, segment, q_ref, k_ref, v_ref, a_ref, f_ref, b_ref, out_ref, map_ref, ka_ref):
    pair = pl.program_id(0)
    rows, width = q_ref.shape
    blocks = rows // segment
    per = width // head_dim
    shift = segment.bit_length() - 1
    row = lax.broadcasted_iota(jnp.int32, (rows, rows), 0)
    col = lax.broadcasted_iota(jnp.int32, (rows, rows), 1)
    same = (row >> shift) == (col >> shift)
    strict = same & (row > col)
    inclusive = same & (row >= col)
    triangle = jnp.where(inclusive, 1.0, 0.0).astype(BF16)
    lane = lax.broadcasted_iota(jnp.int32, (rows, width), 1)
    bias = b_ref[...]
    bias_lane = lax.broadcasted_iota(jnp.int32, bias.shape, 1)

    def spread(values):
        total = values[per - 1]
        for h in range(per - 2, -1, -1):
            total = jnp.where(lane < (h + 1) * head_dim, values[h], total)
        return total

    own_bias = [
        jnp.sum(jnp.where(bias_lane == pair * per + h, bias, 0.0), axis=1, keepdims=True)
        for h in range(per)
    ]
    decay = -(0.6065306597126334 / (1.0 + jnp.exp(-f_ref[...]))) + spread(own_bias)
    high, low = halves(decay)
    lowest = (decay - high.astype(F32) - low.astype(F32)).astype(BF16)
    cumulative = dot(triangle, high) + (dot(triangle, low) + dot(triangle, lowest))
    closing_rows = cumulative.reshape(blocks, segment, width)[:, segment - 1 :, :]
    closing = jnp.broadcast_to(closing_rows, (blocks, segment, width)).reshape(rows, width)
    keys = k_ref[...].astype(F32)
    squares = keys * keys
    norms = spread(
        [
            jnp.sum(squares[:, h * head_dim : (h + 1) * head_dim], axis=1, keepdims=True)
            for h in range(per)
        ]
    )
    removal = keys * lax.rsqrt(norms + 1e-06)
    rate = 1.0 / (1.0 + jnp.exp(-a_ref[...].astype(F32)))
    beta = removal * rate
    grow = jnp.exp(-cumulative)
    fade = jnp.exp(closing - cumulative)
    alpha_all = -removal * jnp.exp(cumulative - decay)
    beta_hat_all = beta * grow
    key_hat_all = keys * grow
    query_all = q_ref[...].astype(F32) * jnp.exp(cumulative)
    beta_bar_all = beta * fade
    key_bar_all = keys * fade
    values_all = v_ref[...]
    keep_all = jnp.exp(closing_rows)
    eye = lax.broadcasted_iota(jnp.int32, (head_dim, head_dim), 0) == lax.broadcasted_iota(
        jnp.int32, (head_dim, head_dim), 1
    )
    outs, maps = [], []
    for h in range(per):
        part = slice(h * head_dim, (h + 1) * head_dim)
        alpha, beta_hat, key_hat = alpha_all[:, part], beta_hat_all[:, part], key_hat_all[:, part]
        query, values = query_all[:, part], values_all[:, part]
        beta_bar, key_bar = beta_bar_all[:, part], key_bar_all[:, part]
        lower = jnp.where(strict, dot3(alpha, beta_hat, (1, 1)), 0.0)
        remove_write = jnp.where(strict, dot3(alpha, key_hat, (1, 1)), 0.0)
        read_remove = jnp.where(inclusive, dot1(query, beta_hat, (1, 1)), 0.0)
        read_write = jnp.where(inclusive, dot1(query, key_hat, (1, 1)), 0.0)
        inverse = jnp.where(row == col, 1.0, jnp.where((row >> 1) == (col >> 1), lower, 0.0))
        for s in range(1, shift):
            off = ((row >> (s + 1)) == (col >> (s + 1))) & ((row >> s) != (col >> s))
            inverse = inverse + dot3(inverse, dot3(jnp.where(off, lower, 0.0), inverse))
        wh, wl = halves(remove_write)
        side = jnp.concatenate([alpha, dot(wh, values) + dot(wl, values)], axis=1)
        solved = dot3(inverse, side)
        read = dot1(read_remove, solved)
        read_map = query + read[:, :head_dim]
        local = read[:, head_dim:] + dot(read_write.astype(BF16), values)
        state = jnp.concatenate(
            [jnp.where(eye, 1.0, 0.0), jnp.zeros((head_dim, head_dim), F32)], axis=0
        )
        out_rows, map_rows = [], []
        for b in range(blocks):
            at = slice(b * segment, (b + 1) * segment)
            seen = dot1(read_map[at], state, (1, 1))
            map_rows.append(seen[:, :head_dim])
            out_rows.append(local[at] + seen[:, head_dim:])
            step = dot3(solved[at], beta_bar[at], (0, 0))
            bh, bl = halves(key_bar[at])
            add = step[head_dim:] + dot(values[at], bh, (0, 0)) + dot(values[at], bl, (0, 0))
            keep = step[:head_dim] + jnp.where(eye, keep_all[b][:, part], 0.0)
            state = dot3(state, keep)
            state = jnp.concatenate([state[:head_dim], state[head_dim:] + add], axis=0)
        outs.append(jnp.concatenate(out_rows, axis=0))
        maps.append(jnp.concatenate(map_rows, axis=0))
        ka_ref[h] = jnp.concatenate([state[:head_dim], state[head_dim:]], axis=1).astype(BF16)
    out_ref[...] = jnp.concatenate(outs, axis=1)
    map_ref[...] = jnp.concatenate(maps, axis=1).astype(BF16)


def exchange_kernel(count, per, workers, ka_ref, st_ref, got, fold, send1, recv1, send2, recv2):
    me = lax.axis_index("sp")
    dim = ka_ref.shape[1]
    barrier = pltpu.get_barrier_semaphore()
    for d in range(1, count):
        pl.semaphore_signal(
            barrier, inc=1, device_id={"sp": lax.rem(me + d, count)}, device_id_type=MESH
        )
    pl.semaphore_wait(barrier, count - 1)

    def first(t, owner):
        return pltpu.make_async_remote_copy(
            src_ref=ka_ref.at[pl.ds(t * per, per)],
            dst_ref=got.at[owner],
            send_sem=send1.at[t],
            recv_sem=recv1.at[owner],
            device_id={"sp": t},
            device_id_type=MESH,
        )

    def second(t, owner):
        return pltpu.make_async_remote_copy(
            src_ref=fold.at[t],
            dst_ref=st_ref.at[pl.ds(owner * per, per)],
            send_sem=send2.at[t],
            recv_sem=recv2.at[owner],
            device_id={"sp": t},
            device_id_type=MESH,
        )

    for t in range(workers):
        @pl.when(t != me)
        def _(t=t):
            first(t, me).start()

    def work():
        got[me] = ka_ref[pl.ds(me * per, per)]
        state = [jnp.zeros((dim, dim), F32) for _ in range(per)]
        for j in range(count):
            @pl.when(j != me)
            def _(j=j):
                pltpu.make_async_remote_copy(
                    src_ref=got.at[j],
                    dst_ref=got.at[j],
                    send_sem=send1.at[0],
                    recv_sem=recv1.at[j],
                    device_id={"sp": j},
                    device_id_type=MESH,
                ).wait_recv()
            for i in range(per):
                fold[j, i] = jnp.concatenate([state[i], jnp.zeros_like(state[i])], axis=1).astype(BF16)
                both = got[j, i]
                keep, add = both[:, :dim], both[:, dim:].astype(F32)
                sh, sl = halves(state[i])
                state[i] = dot(sh, keep) + dot(sl, keep) + add
        for t in range(count):
            @pl.when(t != me)
            def _(t=t):
                second(t, me).start()
        st_ref[pl.ds(me * per, per)] = fold[me]
        for t in range(count):
            @pl.when(t != me)
            def _(t=t):
                second(t, me).wait_send()

    if workers == count:
        work()
    else:
        pl.when(me < workers)(work)
    for t in range(workers):
        @pl.when(t != me)
        def _(t=t):
            first(t, me).wait_send()
            pltpu.make_async_remote_copy(
                src_ref=fold.at[t],
                dst_ref=st_ref.at[pl.ds(t * per, per)],
                send_sem=send2.at[0],
                recv_sem=recv2.at[t],
                device_id={"sp": t},
                device_id_type=MESH,
            ).wait_recv()


def finish_kernel(head_dim, out_ref, map_ref, st_ref, gain_ref, w_ref, part_ref, mixed):
    @pl.when(pl.program_id(0) == 0)
    def _():
        for h in range(out_ref.shape[1] // head_dim):
            part = slice(h * head_dim, (h + 1) * head_dim)
            states = st_ref[h][:, :head_dim]
            output = out_ref[:, part] + dot(map_ref[:, part], states, (1, 1))
            centered = output - jnp.mean(output, axis=1, keepdims=True)
            spread = jnp.mean(centered * centered, axis=1, keepdims=True)
            mixed[:, part] = (centered * lax.rsqrt(spread + 0.00064) * gain_ref[:, part]).astype(BF16)

    part_ref[...] = dot(mixed[...], w_ref[...]).astype(BF16)


def mixer_branch(query, key, value, step, forget, bias, gain, blender):
    count = lax.axis_size("sp")
    rows, channels = query.shape
    heads = bias.shape[1]
    head_dim = channels // heads
    segment = min(64, rows)
    width = 2 * head_dim
    pairs = heads // 2
    block = pl.BlockSpec((rows, width), lambda p: (0, p))
    out, maps, ka = pl.pallas_call(
        functools.partial(mixer_kernel, head_dim, segment),
        grid=(pairs,),
        in_specs=[block] * 5 + [pl.BlockSpec((rows, heads), lambda p: (0, 0))],
        out_specs=[block, block, pl.BlockSpec((2, head_dim, width), lambda p: (p, 0, 0))],
        out_shape=[
            jax.ShapeDtypeStruct((rows, channels), F32),
            jax.ShapeDtypeStruct((rows, channels), BF16),
            jax.ShapeDtypeStruct((heads, head_dim, width), BF16),
        ],
        compiler_params=pltpu.CompilerParams(vmem_limit_bytes=50 * 1024 * 1024),
    )(query, key, value, step, forget, bias)
    per = max(1, heads // count)
    workers = heads // per
    vmem = pl.BlockSpec(memory_space=pltpu.VMEM)
    states = pl.pallas_call(
        functools.partial(exchange_kernel, count, per, workers),
        out_shape=jax.ShapeDtypeStruct((heads, head_dim, width), BF16),
        in_specs=[vmem],
        out_specs=vmem,
        scratch_shapes=[
            pltpu.VMEM((count, per, head_dim, width), BF16),
            pltpu.VMEM((count, per, head_dim, width), BF16),
            pltpu.SemaphoreType.DMA((count,)),
            pltpu.SemaphoreType.DMA((count,)),
            pltpu.SemaphoreType.DMA((count,)),
            pltpu.SemaphoreType.DMA((count,)),
        ],
        compiler_params=pltpu.CompilerParams(collective_id=1, has_side_effects=True),
    )(ka)
    model_width = blender.shape[1]
    tile = min(512, model_width)
    whole = lambda *shape: pl.BlockSpec(shape, lambda p: (0,) * len(shape))
    return pl.pallas_call(
        functools.partial(finish_kernel, head_dim),
        grid=(model_width // tile,),
        in_specs=[
            whole(rows, channels),
            whole(rows, channels),
            whole(heads, head_dim, width),
            whole(1, channels),
            pl.BlockSpec((channels, tile), lambda p: (0, p)),
        ],
        out_specs=pl.BlockSpec((rows, tile), lambda p: (0, p)),
        out_shape=jax.ShapeDtypeStruct((rows, model_width), BF16),
        scratch_shapes=[pltpu.VMEM((rows, channels), BF16)],
    )(out, maps, states, gain.reshape(1, channels), blender)


def body(
    readout_query_vectors,
    attention_key_vectors,
    attention_content_vectors,
    step_size_preactivation,
    forgetting_preactivation,
    extra_forgetting_bias,
    subspace_normalizer_gain,
    skip_connection_stream,
    blender_projection_matrix,
    specialist_prenormal_gain,
    cluster_router_chance,
    specialist_chance_within_cluster,
    chosen_specialist_ids,
    specialist_switch_matrix,
    specialist_expansion_matrix,
    specialist_contraction_matrix,
):
    partial_branch = mixer_branch(
        readout_query_vectors,
        attention_key_vectors,
        attention_content_vectors,
        step_size_preactivation,
        forgetting_preactivation,
        extra_forgetting_bias,
        subspace_normalizer_gain,
        blender_projection_matrix,
    )
    branch = lax.psum(partial_branch, "tp").astype(jnp.float32)
    hidden_state = skip_connection_stream.astype(jnp.float32) + branch
    inverse_rms = lax.rsqrt(jnp.mean(hidden_state * hidden_state, axis=1, keepdims=True) + 1e-06)
    normed = (hidden_state * inverse_rms * specialist_prenormal_gain).astype(jnp.bfloat16)
    tok_rows = skip_connection_stream.shape[0]
    model_width = skip_connection_stream.shape[1]
    local_experts = specialist_switch_matrix.shape[0]
    experts = local_experts * lax.axis_size("sp")
    top_count = chosen_specialist_ids.shape[1]
    capacity = 2 * tok_rows * top_count // experts
    flat_expert = chosen_specialist_ids.reshape(-1)
    one_hot = (flat_expert[:, None] == jnp.arange(experts, dtype=jnp.int32)[None, :]).astype(
        jnp.int32
    )
    earlier = jnp.sum((jnp.cumsum(one_hot, axis=0) - one_hot) * one_hot, axis=1)
    slot_index = flat_expert * capacity + earlier
    token_of = jnp.arange(flat_expert.shape[0], dtype=jnp.int32) // top_count
    slot_owner = jnp.full((experts * capacity,), tok_rows, jnp.int32).at[slot_index].set(token_of)
    padded = jnp.concatenate([normed, jnp.zeros((1, model_width), jnp.bfloat16)], axis=0)
    outgoing = padded[slot_owner].reshape(experts, capacity, model_width)
    route_weight = (
        cluster_router_chance[:, None]
        * specialist_chance_within_cluster
        / jnp.sum(specialist_chance_within_cluster, axis=1, keepdims=True)
    )
    rows_in = lax.all_to_all(outgoing, "sp", split_axis=0, concat_axis=0, tiled=True)
    grouped = rows_in.reshape(-1, local_experts, rows_in.shape[1], model_width)
    gate_act = jnp.einsum(
        "secd,edf->secf", grouped, specialist_switch_matrix, preferred_element_type=jnp.float32
    )
    upward = jnp.einsum(
        "secd,edf->secf", grouped, specialist_expansion_matrix, preferred_element_type=jnp.float32
    )
    hidden = (jax.nn.silu(gate_act) * upward).astype(jnp.bfloat16)
    partial_value = jnp.einsum(
        "secf,efd->secd", hidden, specialist_contraction_matrix, preferred_element_type=jnp.float32
    )
    partial_value = partial_value.astype(jnp.bfloat16).reshape(rows_in.shape)
    summed = lax.psum_scatter(
        partial_value.astype(jnp.float32).astype(jnp.bfloat16),
        "tp",
        scatter_dimension=2,
        tiled=True,
    ).astype(jnp.float32)
    returned = lax.all_to_all(
        summed.astype(jnp.bfloat16), "sp", split_axis=0, concat_axis=0, tiled=True
    ).astype(summed.dtype)
    column_count = returned.shape[2]
    picked = returned.reshape(experts * capacity, column_count)[slot_index].reshape(
        tok_rows, top_count, column_count
    )
    mixture = jnp.sum(route_weight[:, :, None] * picked, axis=1)
    own_columns = lax.dynamic_slice_in_dim(
        hidden_state, lax.axis_index("tp") * column_count, column_count, 1
    )
    return lax.all_gather((own_columns + mixture).astype(jnp.bfloat16), "tp", axis=1, tiled=True)


def solution(mesh):
    in_specs = (
        P("sp", "tp"),
        P("sp", "tp"),
        P("sp", "tp"),
        P("sp", "tp"),
        P("sp", "tp"),
        P("sp", "tp"),
        P("tp"),
        P("sp", None),
        P("tp", None),
        P(),
        P("sp"),
        P("sp", None),
        P("sp", None),
        P("sp", None, "tp"),
        P("sp", None, "tp"),
        P("sp", "tp", None),
    )
    out_specs = P("sp", None)
    return jax.shard_map(body, mesh=mesh, in_specs=in_specs, out_specs=out_specs, check_vma=False)
```

time: 668 us -> 354 us (0.53); the launches traced: 656 us -> 353 us
  other arithmetic: 192 us -> 11 us
  blocking collectives: 170 us -> 98.6 us
  Pallas kernels: 0 us -> 70.5 us
  local copies, waits for them, and re-layouts: 94.1 us -> 25.3 us
  matrix products: 63.1 us -> 15.9 us
    another operation x8 -> x2, other arithmetic: 163 us -> 1.18 us  [the longest x3 159 us: token_mixer_layer(): jax.scipy.linalg.solve_triangular(system, right_side, lower=True, unit_di...]
    all_gather x2 -> x0, blocking collectives: 71.7 us -> none  [carried_in(): lax.all_gather(part.astype(kind), axis)]
    pallas_call x0 -> x3, Pallas kernels: none -> 70.5 us  [the longest x1 45.7 us: mixer_branch(): pl.pallas_call(functools.partial(mixer_kernel, head_dim, segment), grid=(...]
    dot_general x28 -> x0, matrix products: 47.3 us -> none  [the longest x4 13 us: inner_pairs(): return jnp.einsum('bhsd,bhtd->bhst', left, right, precision=HIGH)]
    slice x7 -> x1, local copies, waits for them, and re-layouts: 19.1 us -> 0.21 us  [the longest x1 9.25 us: token_mixer_layer(): keep_before = jnp.concatenate([identity[0][None], keep_prefix[:-1]], axis=0)]
    pad x2 -> x0, local copies, waits for them, and re-layouts: 18.4 us -> none  [token_mixer_layer(): lax.associative_scan(compose, (keep_block, add_block), axis=0)]
    unnamed x70 -> x35, local copies, waits for them, and re-layouts: 22.7 us -> 10.4 us
    dynamic_slice x16 -> x0, local copies, waits for them, and re-layouts: 8.36 us -> none  [hop(): part[k].astype(own.dtype)]
where the time goes in v1:
time: 354 us; the launch traced here: 353 us
  waiting for transfers between devices  113 us (32%)
  blocking collectives  98.6 us (28%)
  Pallas kernels  70.5 us (20%)
  local copies, waits for them, and re-layouts  25.3 us (7%)
  matrix products  15.9 us (4%)
  between operations  13.4 us (4%)
  other arithmetic  11 us (3%)
  starting transfers between devices  5.58 us (2%)
    all_to_all x1, blocking collectives, body(): lax.all_to_all(outgoing, 'sp', split_axis=0, concat_axis=0, tiled=True)  98.6 us
    pallas_call x1, Pallas kernels, mixer_branch(): pl.pallas_call(functools.partial(mixer_kernel, head_dim, segment), grid=(...  45.7 us
    reduce_scatter x1, waiting for transfers between devices, body(): lax.psum_scatter(partial_value.astype(jnp.float32).astype(jnp.bfloat16),...  43.2 us
    psum x1, waiting for transfers between devices, body(): branch = lax.psum(partial_branch, 'tp').astype(jnp.float32)  29.6 us
    all_to_all x1, waiting for transfers between devices, body(): lax.all_to_all(summed.astype(jnp.bfloat16), 'sp', split_axis=0, concat_ax...  25.4 us
    pallas_call x1, Pallas kernels, mixer_branch(): pl.pallas_call(functools.partial(exchange_kernel, count, per, workers), o...  17.9 us
    all_gather x1, waiting for transfers between devices, body(): lax.all_gather((own_columns + mixture).astype(jnp.bfloat16), 'tp', axis=1...  14.9 us
    unnamed x35, local copies, waits for them, and re-layouts  10.4 us
  transfers between devices with their start and end apart: 4, of which 4 were waited for; matrix products, arithmetic and copies ran while one was open for 1% of the time, Pallas kernels for 0%

profile of v1, /device:TPU:0, one launch (start us, length us, event | category | flops | bytes accessed | tf_op | source)
XLA Modules:
  0.0 353.4 jit_solution(4248516650168137709)
XLA Ops:
  6.5 0.0 copy-start
  6.5 0.0 all-reduce.3.cloned.1.call-start
  6.5 1.0 copy.19.b_ref
  7.5 0.0 copy-start.2
  7.5 1.0 copy-done.2
  8.6 0.0 copy-start.4
  8.6 0.9 copy-done.4
  9.5 0.0 copy-start.5
  9.5 0.9 copy-done.5
  10.5 0.9 copy-done.6
  11.4 0.9 copy-done.7
  12.4 45.7 %shard_map.154 = (f32[256,512]{1,0:T(8,128)S(1)}, bf16[256,512]{1,0:T(8,128)(2,1)S(1)}, bf16[8,64,128]{2,1,0:T(8,128)(2,1)S(1)}) custom-call(bf16[256,512]{1,0:T(8,128)(2,1)S(1)} %copy-done.4, bf16[256,512]{1,0:T(8,128)(2,1)S(1)} %copy-done.5, bf16[256,512]{1,0:T(8,128)(2,1)S(1)} %copy-done.6, bf16[256,512]{1,0:T(8,128)(2,1)S(1)} %copy-done.7, ...), custom_call_target="tpu_custom_call" | custom-call | tf_op jit(solution)/shard_map/pallas_call | solution.py:240
  58.1 0.0 copy-start.1
  58.1 0.8 copy-done.1
  58.9 0.7 copy-done.3
  59.6 0.7 copy-done.8
  60.2 17.9 %shard_map.155.st_ref = bf16[8,64,128]{2,1,0:T(8,128)(2,1)} custom-call(bf16[8,64,128]{2,1,0:T(8,128)(2,1)} %copy-done.8), custom_call_target="tpu_custom_call" | custom-call | tf_op jit(solution)/shard_map/pallas_call | solution.py:255
  78.1 0.0 copy-start.12
  78.1 0.0 copy-start.9
  78.1 6.9 %shard_map.156 = bf16[256,2048]{1,0:T(8,128)(2,1)} custom-call(f32[256,512]{1,0:T(8,128)} %copy-done.1, bf16[256,512]{1,0:T(8,128)(2,1)} %copy-done.3, bf16[8,64,128]{2,1,0:T(8,128)(2,1)} %shard_map.155.st_ref, f32[1,512]{1,0:T(1,128)} %bitcast.76, bf16[512,2048]{1,0:T(8,128)(2,1)} %w_ref.1), custom_call_target="tpu_custom_call" | custom-call | tf_op jit(solution)/shard_map/pallas_call | solution.py:273
  85.1 0.0 all-reduce.3.cloned.1.call-update
  85.1 0.0 reduce-scatter.2.cloned.1.call-start
  85.1 0.0 copy-done.12
  85.2 0.1 copy.22
  85.3 0.1 eq.29
  85.4 0.1 eq.25
  85.6 1.1 reduce-window.6
  86.8 0.2 slice_reduce_fusion
  87.0 0.1 copy.21
  87.2 0.1 mul.75
  87.3 0.1 fusion.17
  87.4 2.6 scatter_custom_fusion
  90.1 0.0 copy-start.11
  90.1 29.6 %all-reduce.3.cloned.1.call-done = bf16[256,2048]{1,0:T(8,128)(2,1)} async-done(((bf16[256,2048]{1,0:T(8,128)(2,1)}), bf16[256,2048]{1,0:T(8,128)(2,1)}) %all-reduce.3.cloned.1.call-update) | async-done | bytes 1048592 | tf_op jit(solution)/shard_map/psum | solution.py:317
  119.7 0.0 copy-done.9
  119.7 3.0 convert_add_fusion
  122.8 0.0 copy-done.11
  122.8 0.0 copy-done.10
  122.8 0.5 multiply_convert_fusion
  123.3 0.1 concatenate.3
  123.4 6.0 %gather_fusion = bf16[1024,2048]{1,0:T(8,128)(2,1)} fusion(bf16[257,2048]{1,0:T(8,128)(2,1)S(1)} %concatenate.3, s32[1024]{0:T(1024)S(1)} %fusion.19), kind=kCustom, calls=%fused_computation | custom fusion | bytes 8392704 | tf_op jit(solution)/shard_map/gather | solution.py:336
  129.4 98.6 %all_to_all.10 = bf16[8,128,2048]{2,1,0:T(8,128)(2,1)} all-to-all(bf16[8,128,2048]{2,1,0:T(8,128)(2,1)} %bitcast.72), channel_id=1, replica_groups=mesh['sp'=8,'tp'=4] {'sp'}, dimensions={0} | all-to-all | bytes 8388608 | tf_op jit(solution)/shard_map/all_to_all | solution.py:342
  228.0 0.0 copy-done.15
  228.0 5.8 %fusion.2 = f32[8,128,512]{2,1,0:T(8,128)} fusion(bf16[8,128,2048]{2,1,0:T(8,128)(2,1)} %all_to_all.10, bf16[1,2048,512]{2,1,0:T(8,128)(2,1)S(1)} %copy-done.15), kind=kOutput, calls=%fused_computation.7 | convolution fusion | flops 2147483648 | bytes 8388608 | tf_op jit(solution)/shard_map/secd,edf->secf/dot_general | solution.py:347
  233.8 0.0 copy-done
  233.8 10.1 %convolution_convert_fusion = bf16[8,128,2048]{2,1,0:T(8,128)(2,1)} fusion(bf16[1,512,2048]{2,1,0:T(8,128)(2,1)S(1)} %copy-done, f32[8,128,512]{2,1,0:T(8,128)} %fusion.2, bf16[8,128,2048]{2,1,0:T(8,128)(2,1)} %all_to_all.10, bf16[1,2048,512]{2,1,0:T(8,128)(2,1)} %param.29), kind=kOutput, calls=%fused_computation.3 | convolution fusion | flops 4300210176 | bytes 14680064 | tf_op jit(solution)/shard_map/secf,efd->secd/dot_general | solution.py:351
  243.9 0.0 reduce-scatter.2.cloned.1.call-update
  243.9 0.0 copy-start.13
  243.9 0.0 copy-start.14
  243.9 43.2 %reduce-scatter.2.cloned.1.call-done = bf16[8,128,512]{2,1,0:T(8,128)(2,1)} async-done(((bf16[8,128,2048]{2,1,0:T(8,128)(2,1)}), bf16[8,128,512]{2,1,0:T(8,128)(2,1)}) %reduce-scatter.2.cloned.1.call-update) | async-done | bytes 1048592 | tf_op jit(solution)/shard_map/reduce_scatter | solution.py:355
  287.2 5.5 %all-to-all-start.1 = ((bf16[8,128,512]{2,1,0:T(8,128)(2,1)}), bf16[8,128,512]{2,1,0:T(8,128)(2,1)S(1)}, u32[]{:S(2)}, u32[]{:S(2)}) async-start(bf16[8,128,512]{2,1,0:T(8,128)(2,1)} %reduce-scatter.2.cloned.1.call-done), calls=%async_computation.2 | async-start | bytes 2097152 | tf_op jit(solution)/shard_map/all_to_all | solution.py:361
  292.7 0.0 all-gather.2.cloned.1.call-start
  292.7 0.0 copy-done.13
  292.8 0.0 copy-done.14
  292.8 0.1 copy.20
  293.0 25.4 %all-to-all-done.1 = bf16[8,128,512]{2,1,0:T(8,128)(2,1)S(1)} async-done(((bf16[8,128,512]{2,1,0:T(8,128)(2,1)}), bf16[8,128,512]{2,1,0:T(8,128)(2,1)S(1)}, u32[]{:S(2)}, u32[]{:S(2)}) %all-to-all-start.1) | async-done | bytes 1048608 | tf_op jit(solution)/shard_map/all_to_all | solution.py:361
  318.4 1.7 bitcast_convert_fusion
  320.1 3.6 %gather_fusion.1 = f32[512,512]{1,0:T(8,128)S(1)} fusion(f32[1024,512]{1,0:T(8,128)} %bitcast_convert_fusion, s32[1024]{0:T(1024)S(1)} %pad_clamp_fusion), kind=kCustom, calls=%fused_computation.1 | custom fusion | bytes 2099200 | tf_op jit(solution)/shard_map/gather | solution.py:365
  323.7 1.6 reshape.104
  325.3 2.6 multiply_reduce_fusion.1
  327.9 1.8 add_convert_fusion
  329.7 0.0 all-gather.2.cloned.1.call-update
  329.7 14.9 %all-gather.2.cloned.1.call-done = bf16[256,2048]{1,0:T(8,128)(2,1)} async-done(((bf16[256,512]{1,0:T(8,128)(2,1)}), bf16[256,2048]{1,0:T(8,128)(2,1)}) %all-gather.2.cloned.1.call-update) | async-done | bytes 1048592 | tf_op jit(solution)/shard_map/all_gather | solution.py:372
  344.6 2.3 copy.26
  (17 shorter events, 0.1 us)
Async XLA Ops:
  6.5 227.3 %copy-start = (bf16[1,512,2048]{2,1,0:T(8,128)(2,1)S(1)}, bf16[1,512,2048]{2,1,0:T(8,128)(2,1)}, u32[]{:S(2)}) copy-start(bf16[1,512,2048]{2,1,0:T(8,128)(2,1)} %param.31) | copy-start | bytes 6291460
  6.5 113.2 %all-reduce.3.cloned.1.call-start = ((), (), s32[]{:S(2)}) async-start(), calls=%async_computation.3 | async-start | bytes 2097152 | tf_op jit(solution)/shard_map/psum | solution.py:317
  7.5 1.0 copy-start.2
  8.6 0.9 copy-start.4
  9.5 0.9 copy-start.5
  10.5 0.9 copy-start.6
  11.4 0.9 copy-start.7
  58.1 0.8 copy-start.1
  58.9 0.7 copy-start.3
  59.6 0.7 copy-start.8
  78.1 7.0 %copy-start.12 = (s32[256,2]{0,1:T(2,128)S(1)}, s32[256,2]{0,1:T(2,128)}, u32[]{:S(2)}) copy-start(s32[256,2]{0,1:T(2,128)} %param.28) | copy-start | bytes 6148
  78.1 41.6 %copy-start.9 = (bf16[256,2048]{1,0:T(8,128)(2,1)S(1)}, bf16[256,2048]{1,0:T(8,128)(2,1)}, u32[]{:S(2)}) copy-start(bf16[256,2048]{1,0:T(8,128)(2,1)} %param.23) | copy-start | bytes 3145732
  85.1 202.1 %reduce-scatter.2.cloned.1.call-start = ((), (), s32[]{:S(2)}) async-start(), calls=%async_computation.4 | async-start | bytes 5242880 | tf_op jit(solution)/shard_map/reduce_scatter | solution.py:355
  90.1 32.7 %copy-start.11 = (f32[2048]{0:T(1024)S(1)}, f32[2048]{0:T(1024)}, u32[]{:S(2)}) copy-start(f32[2048]{0:T(1024)} %param.25) | copy-start | bytes 24580
  119.7 3.1 copy-start.10
  129.4 98.6 %copy-start.15 = (bf16[1,2048,512]{2,1,0:T(8,128)(2,1)S(1)}, bf16[1,2048,512]{2,1,0:T(8,128)(2,1)}, u32[]{:S(2)}) copy-start(bf16[1,2048,512]{2,1,0:T(8,128)(2,1)} %param.30) | copy-start | bytes 6291460
  243.9 48.8 %copy-start.13 = (f32[256,2]{0,1:T(2,128)S(1)}, f32[256,2]{0,1:T(2,128)}, u32[]{:S(2)}) copy-start(f32[256,2]{0,1:T(2,128)} %param.27) | copy-start | bytes 6148
  243.9 48.8 %copy-start.14 = (f32[256]{0:T(256)S(1)}, f32[256]{0:T(256)}, u32[]{:S(2)}) copy-start(f32[256]{0:T(256)} %param.26) | copy-start | bytes 3076
  287.2 31.2 %all-to-all-start.1 = ((bf16[8,128,512]{2,1,0:T(8,128)(2,1)}), bf16[8,128,512]{2,1,0:T(8,128)(2,1)S(1)}, u32[]{:S(2)}, u32[]{:S(2)}) async-start(bf16[8,128,512]{2,1,0:T(8,128)(2,1)} %reduce-scatter.2.cloned.1.call-done), calls=%async_computation.2 | async-start | bytes 2097152 | tf_op jit(solution)/shard_map/all_to_all | solution.py:361
  292.7 51.9 %all-gather.2.cloned.1.call-start = ((), (), s32[]{:S(2)}) async-start(), calls=%async_computation.5 | async-start | bytes 1310720 | tf_op jit(solution)/shard_map/all_gather | solution.py:372
Sparse Core Ops, SparseCore 0:
  85.2 34.4 all-reduce.2
  244.0 43.1 reduce-scatter.1
  329.8 14.7 all-gather.1

commit v2 on v1

--- a/solution.py
+++ b/solution.py
@@ -286,6 +286,352 @@
     )(out, maps, states, gain.reshape(1, channels), blender)
 
 
+def greet(sp_count, tp_count, sp, tp):
+    barrier = pltpu.get_barrier_semaphore()
+    for d in range(1, sp_count):
+        pl.semaphore_signal(
+            barrier, inc=1, device_id={"sp": lax.rem(sp + d, sp_count)}, device_id_type=MESH
+        )
+    for d in range(1, tp_count):
+        pl.semaphore_signal(
+            barrier, inc=1, device_id={"tp": lax.rem(tp + d, tp_count)}, device_id_type=MESH
+        )
+    pl.semaphore_wait(barrier, sp_count + tp_count - 2)
+
+
+def copy_to(src, dst, send, recv, device):
+    return pltpu.make_async_remote_copy(
+        src_ref=src,
+        dst_ref=dst,
+        send_sem=send,
+        recv_sem=recv,
+        device_id=device,
+        device_id_type=MESH,
+    )
+
+
+def span(index, size):
+    return pl.ds(pl.multiple_of(index * size, size), size)
+
+
+def row_total(data, terms):
+    ones = jnp.ones((8, data.shape[1]), BF16)
+    total = None
+    for _ in range(terms):
+        piece = data.astype(BF16)
+        data = data - piece.astype(F32)
+        product = dot(ones, piece, (1, 1))
+        total = product if total is None else total + product
+    return total
+
+
+def route_kernel(
+    sp_count, tp_count, experts, capacity,
+    part_ref, skip_ref, gain_ref, ids_ref,
+    hidden_ref, slot_ref, rows_ref,
+    gathered, squares, outgoing,
+    s_part, r_part, s_sq, r_sq, s_out, r_out, s_own, s_fwd, r_col,
+):
+    sp, tp = lax.axis_index("sp"), lax.axis_index("tp")
+    rows, model = part_ref.shape
+    cols = model // tp_count
+    mine = span(tp, cols)
+    groups = tp_count // 2
+    core, group = lax.rem(tp, 2), tp // 2
+    sibling = group * 2 + 1 - core
+    greet(sp_count, tp_count, sp, tp)
+
+    def part_copy(p):
+        return copy_to(
+            part_ref.at[:, span(p, cols)], gathered.at[tp], s_part.at[p], r_part.at[tp], {"tp": p}
+        )
+
+    for d in range(1, tp_count):
+        part_copy(lax.rem(tp + d, tp_count)).start()
+
+    ids = ids_ref[...]
+    top = ids.shape[1]
+    lanes = lax.broadcasted_iota(jnp.int32, (rows, experts), 1)
+    named = [ids[:, k : k + 1] == lanes for k in range(top)]
+    anyone = sum(jnp.where(n, 1.0, 0.0) for n in named).astype(BF16)
+    r0 = lax.broadcasted_iota(jnp.int32, (rows, rows), 0)
+    r1 = lax.broadcasted_iota(jnp.int32, (rows, rows), 1)
+    before = dot(jnp.where(r0 > r1, 1.0, 0.0).astype(BF16), anyone)
+    slots = [
+        jnp.sum(
+            jnp.where(n, before + lanes.astype(F32) * capacity, 0.0), axis=1, keepdims=True
+        ).astype(jnp.int32)
+        for n in named
+    ]
+    slot_ref[...] = jnp.concatenate(slots, axis=1)
+
+    branch = part_ref[:, mine].astype(F32)
+    for d in range(1, tp_count):
+        p = lax.rem(tp + d, tp_count)
+        copy_to(gathered.at[p], gathered.at[p], s_part.at[p], r_part.at[p], {"tp": p}).wait_recv()
+        branch = branch + gathered[p].astype(F32)
+    hidden = skip_ref[:, mine].astype(F32) + branch
+    hidden_ref[...] = hidden
+    squares[tp] = row_total(hidden * hidden, 3)
+
+    def square_copy(p):
+        return copy_to(squares.at[tp], squares.at[tp], s_sq.at[p], r_sq.at[tp], {"tp": p})
+
+    for d in range(1, tp_count):
+        square_copy(lax.rem(tp + d, tp_count)).start()
+    total = squares[tp]
+    for d in range(1, tp_count):
+        p = lax.rem(tp + d, tp_count)
+        copy_to(squares.at[p], squares.at[p], s_sq.at[p], r_sq.at[p], {"tp": p}).wait_recv()
+        total = total + squares[p]
+    inverse = lax.rsqrt(total / model + 1e-06)
+    first = jnp.where(lax.broadcasted_iota(jnp.int32, (8, 128), 0) == 0, 1.0, 0.0).astype(BF16)
+    column = None
+    for _ in range(3):
+        piece = inverse.astype(BF16)
+        inverse = inverse - piece.astype(F32)
+        product = dot(piece, first, (0, 0))
+        column = product if column is None else column + product
+    normed = (hidden * column[:, :1] * gain_ref[:, mine]).astype(BF16)
+
+    per = experts // sp_count * capacity
+    places = lax.broadcasted_iota(jnp.int32, (rows, per), 1)
+
+    def block_for(t):
+        at = places + t * per
+        chosen = (slots[0] == at)
+        for s in slots[1:]:
+            chosen = chosen | (s == at)
+        return dot(jnp.where(chosen, 1.0, 0.0).astype(BF16), normed, (0, 0)).astype(BF16)
+
+    def out_copy(t):
+        return copy_to(
+            outgoing.at[t], rows_ref.at[sp, :, mine], s_out.at[t], r_out.at[sp], {"sp": t}
+        )
+
+    def give(d, carry):
+        t = lax.rem(sp + d, sp_count)
+        outgoing[t] = block_for(t)
+        out_copy(t).start()
+        return carry
+
+    lax.fori_loop(1, sp_count, give, 0)
+    rows_ref[sp, :, mine] = block_for(sp)
+
+    def own_copy(p, s):
+        here = rows_ref.at[s, :, mine]
+        return copy_to(here, here, s_own.at[p, s], r_col.at[tp, s], {"tp": p})
+
+    def forward(o, s):
+        here = rows_ref.at[s, :, span(o, cols)]
+        return copy_to(here, here, s_fwd.at[o, s], r_col.at[o, s], {"tp": sibling})
+
+    def arrived(o, s):
+        here = rows_ref.at[s, :, span(o, cols)]
+        copy_to(here, here, s_fwd.at[o, s], r_col.at[o, s], {"tp": sibling}).wait_recv()
+
+    def peers():
+        return [lax.rem(group + g, groups) * 2 + core for g in range(1, groups)]
+
+    lag = 2
+
+    def relay(d, carry):
+        @pl.when(d < sp_count)
+        def _():
+            s = lax.rem(sp - d + sp_count, sp_count)
+
+            @pl.when(d > 0)
+            def _():
+                here = rows_ref.at[s, :, mine]
+                copy_to(here, here, s_out.at[s], r_out.at[s], {"sp": s}).wait_recv()
+
+            for p in peers():
+                own_copy(p, s).start()
+            own_copy(sibling, s).start()
+
+        @pl.when(d >= lag)
+        def _():
+            s = lax.rem(sp - (d - lag) + sp_count, sp_count)
+            for o in peers():
+                arrived(o, s)
+                forward(o, s).start()
+
+        return carry
+
+    lax.fori_loop(0, sp_count + lag, relay, 0)
+
+    def settle(s, carry):
+        arrived(sibling, s)
+        for g in range(1, groups):
+            arrived(lax.rem(group + g, groups) * 2 + 1 - core, s)
+        own_copy(sibling, s).wait_send()
+        for p in peers():
+            own_copy(p, s).wait_send()
+            forward(p, s).wait_send()
+        return carry
+
+    lax.fori_loop(0, sp_count, settle, 0)
+
+    def sent(d, carry):
+        out_copy(lax.rem(sp + d, sp_count)).wait_send()
+        return carry
+
+    lax.fori_loop(1, sp_count, sent, 0)
+    for d in range(1, tp_count):
+        p = lax.rem(tp + d, tp_count)
+        part_copy(p).wait_send()
+        square_copy(p).wait_send()
+
+
+def return_kernel(
+    sp_count, tp_count,
+    y_ref, hidden_ref, slot_ref, weight_ref,
+    out_ref,
+    from_sib, pair, from_peer, summed, back,
+    s_sib, r_sib, s_peer, r_peer, s_back, r_back, s_own, s_fwd, r_col,
+):
+    sp, tp = lax.axis_index("sp"), lax.axis_index("tp")
+    per, model = y_ref.shape[1:]
+    rows = hidden_ref.shape[0]
+    cols = model // tp_count
+    mine = span(tp, cols)
+    groups = tp_count // 2
+    core, group = lax.rem(tp, 2), tp // 2
+    sibling = group * 2 + 1 - core
+    greet(sp_count, tp_count, sp, tp)
+
+    def sib_copy(s, g):
+        return copy_to(
+            y_ref.at[s, :, span(g * 2 + 1 - core, cols)],
+            from_sib.at[s, g],
+            s_sib.at[s, g],
+            r_sib.at[s, g],
+            {"tp": sibling},
+        )
+
+    def peer_copy(s, g):
+        return copy_to(
+            pair.at[s, g],
+            from_peer.at[s, group],
+            s_peer.at[s, g],
+            r_peer.at[s, group],
+            {"tp": g * 2 + core},
+        )
+
+    def back_copy(t):
+        return copy_to(summed.at[t], back.at[sp], s_back.at[t], r_back.at[sp], {"sp": t})
+
+    def others():
+        return [lax.rem(group + d, groups) for d in range(1, groups)]
+
+    def order(d):
+        return lax.rem(sp + 1 + d, sp_count)
+
+    def open_up(d, carry):
+        s = order(d)
+        for g in others():
+            sib_copy(s, g).start()
+        sib_copy(s, group).start()
+        return carry
+
+    lax.fori_loop(0, sp_count, open_up, 0)
+    lag = 2
+
+    def step(d, carry):
+        @pl.when(d < sp_count)
+        def _():
+            s = order(d)
+            for g in others():
+                sib_copy(s, g).wait_recv()
+                pair[s, g] = (
+                    y_ref[s, :, span(g * 2 + core, cols)].astype(F32) + from_sib[s, g].astype(F32)
+                ).astype(BF16)
+                peer_copy(s, g).start()
+            sib_copy(s, group).wait_recv()
+
+        @pl.when(d >= lag)
+        def _():
+            s = order(d - lag)
+            total = y_ref[s, :, mine].astype(F32) + from_sib[s, group].astype(F32)
+            for g in others():
+                copy_to(
+                    from_peer.at[s, g],
+                    from_peer.at[s, g],
+                    s_peer.at[s, g],
+                    r_peer.at[s, g],
+                    {"tp": g * 2 + core},
+                ).wait_recv()
+                total = total + from_peer[s, g].astype(F32)
+
+            @pl.when(s != sp)
+            def _():
+                summed[s] = total.astype(BF16)
+                back_copy(s).start()
+
+            @pl.when(s == sp)
+            def _():
+                back[s] = total.astype(BF16)
+
+        return carry
+
+    lax.fori_loop(0, sp_count + lag, step, 0)
+    slots = slot_ref[...]
+    weights = weight_ref[...]
+    places = lax.broadcasted_iota(jnp.int32, (rows, sp_count * per), 1)
+    top = slots.shape[1]
+    chosen = [jnp.where(slots[:, k : k + 1] == places, 1.0, 0.0).astype(BF16) for k in range(top)]
+
+    def landed(d, carry):
+        s = lax.rem(sp + d, sp_count)
+        copy_to(back.at[s], back.at[s], s_back.at[s], r_back.at[s], {"sp": s}).wait_recv()
+        return carry
+
+    lax.fori_loop(1, sp_count, landed, 0)
+    returned = back[...].reshape(sp_count * per, cols)
+    result = hidden_ref[...] + sum(
+        weights[:, k : k + 1] * dot(chosen[k], returned) for k in range(top)
+    )
+    out_ref[:, mine] = result.astype(BF16)
+
+    def own_copy(p):
+        here = out_ref.at[:, mine]
+        return copy_to(here, here, s_own.at[p], r_col.at[tp], {"tp": p})
+
+    def forward(o):
+        here = out_ref.at[:, span(o, cols)]
+        return copy_to(here, here, s_fwd.at[o], r_col.at[o], {"tp": sibling})
+
+    peers = [g * 2 + core for g in others()]
+    for p in peers:
+        own_copy(p).start()
+    own_copy(sibling).start()
+    for p in peers:
+        forward(p).wait_recv()
+        forward(p).start()
+    forward(sibling).wait_recv()
+    for g in others():
+        forward(g * 2 + 1 - core).wait_recv()
+    own_copy(sibling).wait_send()
+    for p in peers:
+        own_copy(p).wait_send()
+        forward(p).wait_send()
+
+    def close(s, carry):
+        sib_copy(s, group).wait_send()
+        for g in others():
+            sib_copy(s, g).wait_send()
+            peer_copy(s, g).wait_send()
+        return carry
+
+    lax.fori_loop(0, sp_count, close, 0)
+
+    def sent(d, carry):
+        back_copy(lax.rem(sp + d, sp_count)).wait_send()
+        return carry
+
+    lax.fori_loop(1, sp_count, sent, 0)
+
+
 def body(
     readout_query_vectors,
     attention_key_vectors,
@@ -314,33 +660,55 @@
         subspace_normalizer_gain,
         blender_projection_matrix,
     )
-    branch = lax.psum(partial_branch, "tp").astype(jnp.float32)
-    hidden_state = skip_connection_stream.astype(jnp.float32) + branch
-    inverse_rms = lax.rsqrt(jnp.mean(hidden_state * hidden_state, axis=1, keepdims=True) + 1e-06)
-    normed = (hidden_state * inverse_rms * specialist_prenormal_gain).astype(jnp.bfloat16)
-    tok_rows = skip_connection_stream.shape[0]
-    model_width = skip_connection_stream.shape[1]
+    tok_rows, model_width = skip_connection_stream.shape
+    sp_count, tp_count = lax.axis_size("sp"), lax.axis_size("tp")
     local_experts = specialist_switch_matrix.shape[0]
-    experts = local_experts * lax.axis_size("sp")
+    experts = local_experts * sp_count
     top_count = chosen_specialist_ids.shape[1]
     capacity = 2 * tok_rows * top_count // experts
-    flat_expert = chosen_specialist_ids.reshape(-1)
-    one_hot = (flat_expert[:, None] == jnp.arange(experts, dtype=jnp.int32)[None, :]).astype(
-        jnp.int32
-    )
-    earlier = jnp.sum((jnp.cumsum(one_hot, axis=0) - one_hot) * one_hot, axis=1)
-    slot_index = flat_expert * capacity + earlier
-    token_of = jnp.arange(flat_expert.shape[0], dtype=jnp.int32) // top_count
-    slot_owner = jnp.full((experts * capacity,), tok_rows, jnp.int32).at[slot_index].set(token_of)
-    padded = jnp.concatenate([normed, jnp.zeros((1, model_width), jnp.bfloat16)], axis=0)
-    outgoing = padded[slot_owner].reshape(experts, capacity, model_width)
+    cols = model_width // tp_count
+    per = local_experts * capacity
+    groups = tp_count // 2
+    vmem = pl.BlockSpec(memory_space=pltpu.VMEM)
+    sems = pltpu.SemaphoreType.DMA
+    hidden_cols, slots, rows_in = pl.pallas_call(
+        functools.partial(route_kernel, sp_count, tp_count, experts, capacity),
+        out_shape=[
+            jax.ShapeDtypeStruct((tok_rows, cols), F32),
+            jax.ShapeDtypeStruct((tok_rows, top_count), jnp.int32),
+            jax.ShapeDtypeStruct((sp_count, per, model_width), BF16),
+        ],
+        in_specs=[vmem] * 4,
+        out_specs=[vmem] * 3,
+        scratch_shapes=[
+            pltpu.VMEM((tp_count, tok_rows, cols), BF16),
+            pltpu.VMEM((tp_count, 8, tok_rows), F32),
+            pltpu.VMEM((sp_count, per, cols), BF16),
+            sems((tp_count,)),
+            sems((tp_count,)),
+            sems((tp_count,)),
+            sems((tp_count,)),
+            sems((sp_count,)),
+            sems((sp_count,)),
+            sems((tp_count, sp_count)),
+            sems((tp_count, sp_count)),
+            sems((tp_count, sp_count)),
+        ],
+        compiler_params=pltpu.CompilerParams(
+            collective_id=2, has_side_effects=True, vmem_limit_bytes=40 * 1024 * 1024
+        ),
+    )(
+        partial_branch,
+        skip_connection_stream,
+        specialist_prenormal_gain.reshape(1, model_width),
+        chosen_specialist_ids,
+    )
     route_weight = (
         cluster_router_chance[:, None]
         * specialist_chance_within_cluster
         / jnp.sum(specialist_chance_within_cluster, axis=1, keepdims=True)
     )
-    rows_in = lax.all_to_all(outgoing, "sp", split_axis=0, concat_axis=0, tiled=True)
-    grouped = rows_in.reshape(-1, local_experts, rows_in.shape[1], model_width)
+    grouped = rows_in.reshape(sp_count, local_experts, capacity, model_width)
     gate_act = jnp.einsum(
         "secd,edf->secf", grouped, specialist_switch_matrix, preferred_element_type=jnp.float32
     )
@@ -352,24 +720,31 @@
         "secf,efd->secd", hidden, specialist_contraction_matrix, preferred_element_type=jnp.float32
     )
     partial_value = partial_value.astype(jnp.bfloat16).reshape(rows_in.shape)
-    summed = lax.psum_scatter(
-        partial_value.astype(jnp.float32).astype(jnp.bfloat16),
-        "tp",
-        scatter_dimension=2,
-        tiled=True,
-    ).astype(jnp.float32)
-    returned = lax.all_to_all(
-        summed.astype(jnp.bfloat16), "sp", split_axis=0, concat_axis=0, tiled=True
-    ).astype(summed.dtype)
-    column_count = returned.shape[2]
-    picked = returned.reshape(experts * capacity, column_count)[slot_index].reshape(
-        tok_rows, top_count, column_count
-    )
-    mixture = jnp.sum(route_weight[:, :, None] * picked, axis=1)
-    own_columns = lax.dynamic_slice_in_dim(
-        hidden_state, lax.axis_index("tp") * column_count, column_count, 1
-    )
-    return lax.all_gather((own_columns + mixture).astype(jnp.bfloat16), "tp", axis=1, tiled=True)
+    return pl.pallas_call(
+        functools.partial(return_kernel, sp_count, tp_count),
+        out_shape=jax.ShapeDtypeStruct((tok_rows, model_width), BF16),
+        in_specs=[vmem] * 4,
+        out_specs=vmem,
+        scratch_shapes=[
+            pltpu.VMEM((sp_count, groups, per, cols), BF16),
+            pltpu.VMEM((sp_count, groups, per, cols), BF16),
+            pltpu.VMEM((sp_count, groups, per, cols), BF16),
+            pltpu.VMEM((sp_count, per, cols), BF16),
+            pltpu.VMEM((sp_count, per, cols), BF16),
+            sems((sp_count, groups)),
+            sems((sp_count, groups)),
+            sems((sp_count, groups)),
+            sems((sp_count, groups)),
+            sems((sp_count,)),
+            sems((sp_count,)),
+            sems((tp_count,)),
+            sems((tp_count,)),
+            sems((tp_count,)),
+        ],
+        compiler_params=pltpu.CompilerParams(
+            collective_id=3, has_side_effects=True, vmem_limit_bytes=50 * 1024 * 1024
+        ),
+    )(partial_value, hidden_cols, slots, route_weight)
 
 
 def solution(mesh):

time: 354 us -> 202 us (0.57)
  waiting for transfers between devices: 113 us -> 0 us
  Pallas kernels: 70.5 us -> 171 us
  blocking collectives: 98.6 us -> 0 us
  between operations: 13.4 us -> 0.16 us
  local copies, waits for them, and re-layouts: 25.3 us -> 13.2 us
  other arithmetic: 11 us -> 0.13 us
  starting transfers between devices: 5.58 us -> 0 us
    pallas_call x0 -> x2, Pallas kernels: none -> 101 us  [the longest x1 52.4 us: body(): pl.pallas_call(functools.partial(route_kernel, sp_count, tp_count, expert...]
    all_to_all x1 -> x0, blocking collectives: 98.6 us -> none  [body(): lax.all_to_all(outgoing, 'sp', split_axis=0, concat_axis=0, tiled=True)]
    reduce_scatter x1 -> x0, waiting for transfers between devices: 43.2 us -> none  [body(): lax.psum_scatter(partial_value.astype(jnp.float32).astype(jnp.bfloat16),...]
    psum x1 -> x0, waiting for transfers between devices: 29.6 us -> none  [body(): branch = lax.psum(partial_branch, 'tp').astype(jnp.float32)]
    all_to_all x1 -> x0, waiting for transfers between devices: 25.4 us -> none  [body(): lax.all_to_all(summed.astype(jnp.bfloat16), 'sp', split_axis=0, concat_ax...]
    all_gather x1 -> x0, waiting for transfers between devices: 14.9 us -> none  [body(): lax.all_gather((own_columns + mixture).astype(jnp.bfloat16), 'tp', axis=1...]
    gather x2 -> x0, local copies, waits for them, and re-layouts: 9.65 us -> none  [the longest x1 6.03 us: body(): outgoing = padded[slot_owner].reshape(experts, capacity, model_width)]
    all_to_all x1 -> x0, starting transfers between devices: 5.5 us -> none  [body(): lax.all_to_all(summed.astype(jnp.bfloat16), 'sp', split_axis=0, concat_ax...]
  transfers between devices with their start and end apart: 4 -> 0, of which waited for: 4 -> 0; matrix products, arithmetic and copies ran while one was open for 1% -> 0% of each run, Pallas kernels for 0% -> 0%
where the time goes in v2:
time: 202 us; the launch traced here: 199 us
  Pallas kernels  171 us (85%)
  matrix products  13.9 us (7%)
  local copies, waits for them, and re-layouts  13.2 us (7%)
    pallas_call x1, Pallas kernels, body(): pl.pallas_call(functools.partial(route_kernel, sp_count, tp_count, expert...  52.4 us
    pallas_call x1, Pallas kernels, body(): pl.pallas_call(functools.partial(return_kernel, sp_count, tp_count), out_...  48.3 us
    pallas_call x1, Pallas kernels, mixer_branch(): pl.pallas_call(functools.partial(mixer_kernel, head_dim, segment), grid=(...  45.7 us
    pallas_call x1, Pallas kernels, mixer_branch(): pl.pallas_call(functools.partial(exchange_kernel, count, per, workers), o...  17.8 us
    unnamed x41, local copies, waits for them, and re-layouts  13 us
    dot_general x1, matrix products, body(): jnp.einsum('secf,efd->secd', hidden, specialist_contraction_matrix, prefe...  10.2 us
    pallas_call x1, Pallas kernels, mixer_branch(): pl.pallas_call(functools.partial(finish_kernel, head_dim), grid=(model_wi...  6.93 us

profile of v2, /device:TPU:0, one launch (start us, length us, event | category | flops | bytes accessed | tf_op | source)
XLA Modules:
  0.0 198.5 jit_solution(8767130774388057471)
XLA Ops:
  0.0 0.0 copy-start
  0.0 1.0 copy.21.b_ref
  1.0 0.0 copy-start.6
  1.0 1.0 copy-done.6
  2.0 0.0 copy-start.8
  2.0 0.9 copy-done.8
  3.0 0.0 copy-start.9
  3.0 0.9 copy-done.9
  3.9 0.0 copy-start.10
  3.9 0.9 copy-done.10
  4.9 0.0 copy-start.11
  4.9 0.9 copy-done.11
  5.8 45.7 %shard_map.154 = (f32[256,512]{1,0:T(8,128)S(1)}, bf16[256,512]{1,0:T(8,128)(2,1)S(1)}, bf16[8,64,128]{2,1,0:T(8,128)(2,1)S(1)}) custom-call(bf16[256,512]{1,0:T(8,128)(2,1)S(1)} %copy-done.8, bf16[256,512]{1,0:T(8,128)(2,1)S(1)} %copy-done.9, bf16[256,512]{1,0:T(8,128)(2,1)S(1)} %copy-done.10, bf16[256,512]{1,0:T(8,128)(2,1)S(1)} %copy-done.11, ...), custom_call_target="tpu_custom_call" | custom-call | tf_op jit(solution)/shard_map/pallas_call | solution.py:240
  51.6 0.0 copy-start.5
  51.6 0.8 copy-done.5
  52.4 0.0 copy-start.7
  52.4 0.7 copy-done.7
  53.1 0.0 copy-start.12
  53.1 0.7 copy-done.12
  53.7 17.8 %shard_map.155.st_ref = bf16[8,64,128]{2,1,0:T(8,128)(2,1)} custom-call(bf16[8,64,128]{2,1,0:T(8,128)(2,1)} %copy-done.12), custom_call_target="tpu_custom_call" | custom-call | tf_op jit(solution)/shard_map/pallas_call | solution.py:255
  71.6 0.0 copy-start.15
  71.6 0.0 copy-start.2
  71.6 0.0 copy-start.13
  71.6 6.9 %shard_map.156.part_ref = bf16[256,2048]{1,0:T(8,128)(2,1)} custom-call(f32[256,512]{1,0:T(8,128)} %copy-done.5, bf16[256,512]{1,0:T(8,128)(2,1)} %copy-done.7, bf16[8,64,128]{2,1,0:T(8,128)(2,1)} %shard_map.155.st_ref, f32[1,512]{1,0:T(1,128)} %bitcast.60, bf16[512,2048]{1,0:T(8,128)(2,1)} %w_ref.1), custom_call_target="tpu_custom_call" | custom-call | tf_op jit(solution)/shard_map/pallas_call | solution.py:273
  78.5 0.0 copy-done.15
  78.5 0.1 copy.22.ids_ref
  78.7 0.0 copy-done.2
  78.7 0.0 copy-done.13
  78.7 0.0 copy-start.1
  78.7 1.2 copy-done.1
  79.9 0.0 copy-start.18
  79.9 52.4 %shard_map.157 = (f32[256,512]{1,0:T(8,128)S(1)}, s32[256,2]{1,0:T(8,128)S(1)}, bf16[8,128,2048]{2,1,0:T(8,128)(2,1)S(1)}) custom-call(bf16[256,2048]{1,0:T(8,128)(2,1)S(1)} %copy-done.1, bf16[256,2048]{1,0:T(8,128)(2,1)S(1)} %copy-done.2, f32[1,2048]{1,0:T(1,128)S(1)} %bitcast.59, s32[256,2]{1,0:T(8,128)S(1)} %copy.22.ids_ref), custom_call_target="tpu_custom_call" | custom-call | tf_op jit(solution)/shard_map/pallas_call | solution.py:674
  132.4 0.0 copy-start.3
  132.4 0.8 copy-done.3
  133.2 0.0 copy-start.14
  133.2 2.0 copy-done.14
  135.1 0.0 copy-done.18
  135.1 3.7 %fusion.2 = f32[8,128,512]{2,1,0:T(8,128)} fusion(bf16[8,128,2048]{2,1,0:T(8,128)(2,1)S(1)} %get-tuple-element.14, bf16[1,2048,512]{2,1,0:T(8,128)(2,1)S(1)} %copy-done.18), kind=kOutput, calls=%fused_computation.4 | convolution fusion | flops 2147483648 | bytes 8388608 | tf_op jit(solution)/shard_map/secd,edf->secf/dot_general | solution.py:715
  138.8 0.0 copy-done
  138.8 0.0 copy-start.16
  138.8 0.0 copy-start.17
  138.8 0.0 copy-start.4
  138.8 10.2 %convolution_convert_fusion.y_ref = bf16[8,128,2048]{2,1,0:T(8,128)(2,1)} fusion(bf16[1,512,2048]{2,1,0:T(8,128)(2,1)S(1)} %copy-done, f32[8,128,512]{2,1,0:T(8,128)} %fusion.2, bf16[8,128,2048]{2,1,0:T(8,128)(2,1)} %copy-done.14, bf16[1,2048,512]{2,1,0:T(8,128)(2,1)} %param.29), kind=kOutput, calls=%fused_computation | convolution fusion | flops 4300210176 | bytes 14680064 | tf_op jit(solution)/shard_map/secf,efd->secd/dot_general | solution.py:719
  149.0 0.0 copy-done.16
  149.0 0.0 copy-done.17
  149.0 0.1 copy.23
  149.2 0.1 broadcast_divide_fusion.weight_ref
  149.3 0.0 copy-done.4
  149.3 48.3 %shard_map.158 = bf16[256,2048]{1,0:T(8,128)(2,1)S(1)} custom-call(bf16[8,128,2048]{2,1,0:T(8,128)(2,1)} %convolution_convert_fusion.y_ref, f32[256,512]{1,0:T(8,128)S(1)} %copy-done.4, s32[256,2]{1,0:T(8,128)S(1)} %get-tuple-element.16.slot_ref, f32[256,2]{1,0:T(8,128)S(1)} %broadcast_divide_fusion.weight_ref), custom_call_target="tpu_custom_call" | custom-call | tf_op jit(solution)/shard_map/pallas_call | solution.py:723
  197.6 1.0 copy.26
  (1 shorter events, 0.0 us)
Async XLA Ops:
  0.0 138.8 %copy-start = (bf16[1,512,2048]{2,1,0:T(8,128)(2,1)S(1)}, bf16[1,512,2048]{2,1,0:T(8,128)(2,1)}, u32[]{:S(2)}) copy-start(bf16[1,512,2048]{2,1,0:T(8,128)(2,1)} %param.31) | copy-start | bytes 6291460
  1.0 1.0 copy-start.6
  2.0 0.9 copy-start.8
  3.0 0.9 copy-start.9
  3.9 0.9 copy-start.10
  4.9 0.9 copy-start.11
  51.6 0.8 copy-start.5
  52.4 0.7 copy-start.7
  53.1 0.7 copy-start.12
  71.6 7.0 %copy-start.15 = (s32[256,2]{0,1:T(2,128)S(1)}, s32[256,2]{0,1:T(2,128)}, u32[]{:S(2)}) copy-start(s32[256,2]{0,1:T(2,128)} %param.28) | copy-start | bytes 6148
  71.6 7.1 %copy-start.2 = (bf16[256,2048]{1,0:T(8,128)(2,1)S(1)}, bf16[256,2048]{1,0:T(8,128)(2,1)}, u32[]{:S(2)}) copy-start(bf16[256,2048]{1,0:T(8,128)(2,1)} %skip_ref.1) | copy-start | bytes 3145732
  71.6 7.1 %copy-start.13 = (f32[2048]{0:T(1024)S(1)}, f32[2048]{0:T(1024)}, u32[]{:S(2)}) copy-start(f32[2048]{0:T(1024)} %param.25) | copy-start | bytes 24580
  78.7 1.2 copy-start.1
  79.9 55.2 %copy-start.18 = (bf16[1,2048,512]{2,1,0:T(8,128)(2,1)S(1)}, bf16[1,2048,512]{2,1,0:T(8,128)(2,1)}, u32[]{:S(2)}) copy-start(bf16[1,2048,512]{2,1,0:T(8,128)(2,1)} %param.30) | copy-start | bytes 6291460
  132.4 0.8 copy-start.3
  133.2 2.0 copy-start.14
  138.8 10.2 %copy-start.16 = (f32[256,2]{0,1:T(2,128)S(1)}, f32[256,2]{0,1:T(2,128)}, u32[]{:S(2)}) copy-start(f32[256,2]{0,1:T(2,128)} %param.27) | copy-start | bytes 6148
  138.8 10.2 %copy-start.17 = (f32[256]{0:T(256)S(1)}, f32[256]{0:T(256)}, u32[]{:S(2)}) copy-start(f32[256]{0:T(256)} %param.26) | copy-start | bytes 3076
  138.8 10.5 %copy-start.4 = (f32[256,512]{1,0:T(8,128)S(1)}, f32[256,512]{1,0:T(8,128)}, u32[]{:S(2)}) copy-start(f32[256,512]{1,0:T(8,128)} %copy-done.3) | copy-start | bytes 1572868

commit v3 on v2

--- a/solution.py
+++ b/solution.py
@@ -1,4 +1,5 @@
 import functools
+import math
 
 import jax
 import jax.numpy as jnp
@@ -96,16 +97,23 @@
         query, values = query_all[:, part], values_all[:, part]
         beta_bar, key_bar = beta_bar_all[:, part], key_bar_all[:, part]
         lower = jnp.where(strict, dot3(alpha, beta_hat, (1, 1)), 0.0)
-        remove_write = jnp.where(strict, dot3(alpha, key_hat, (1, 1)), 0.0)
+        remove_write = jnp.where(strict, dot1(alpha, key_hat, (1, 1)), 0.0)
         read_remove = jnp.where(inclusive, dot1(query, beta_hat, (1, 1)), 0.0)
         read_write = jnp.where(inclusive, dot1(query, key_hat, (1, 1)), 0.0)
+        lh, ll = halves(lower)
         inverse = jnp.where(row == col, 1.0, jnp.where((row >> 1) == (col >> 1), lower, 0.0))
         for s in range(1, shift):
             off = ((row >> (s + 1)) == (col >> (s + 1))) & ((row >> s) != (col >> s))
-            inverse = inverse + dot3(inverse, dot3(jnp.where(off, lower, 0.0), inverse))
+            near = inverse.astype(BF16)
+            reach = dot(jnp.where(off, lower, 0.0).astype(BF16), near)
+            inverse = inverse + dot(near, reach.astype(BF16))
         wh, wl = halves(remove_write)
         side = jnp.concatenate([alpha, dot(wh, values) + dot(wl, values)], axis=1)
-        solved = dot3(inverse, side)
+        near = inverse.astype(BF16)
+        solved = dot(near, side.astype(BF16))
+        sh, sl = halves(solved)
+        miss = side - solved + (dot(lh, sh) + (dot(lh, sl) + dot(ll, sh)))
+        solved = solved + dot(near, miss.astype(BF16))
         read = dot1(read_remove, solved)
         read_map = query + read[:, :head_dim]
         local = read[:, head_dim:] + dot(read_write.astype(BF16), values)
@@ -485,9 +493,9 @@
 
 def return_kernel(
     sp_count, tp_count,
-    y_ref, hidden_ref, slot_ref, weight_ref,
+    rows_ref, switch_ref, expand_ref, contract_ref, hidden_ref, slot_ref, weight_ref,
     out_ref,
-    from_sib, pair, from_peer, summed, back,
+    y_ref, from_sib, pair, from_peer, summed, back,
     s_sib, r_sib, s_peer, r_peer, s_back, r_back, s_own, s_fwd, r_col,
 ):
     sp, tp = lax.axis_index("sp"), lax.axis_index("tp")
@@ -527,54 +535,74 @@
     def order(d):
         return lax.rem(sp + 1 + d, sp_count)
 
-    def open_up(d, carry):
-        s = order(d)
+    local = switch_ref.shape[0]
+    capacity = per // local
+    chunk = math.gcd(sp_count, max(1, 256 // capacity))
+    chunks = sp_count // chunk
+
+    def expert(i):
+        at = [order(i * chunk + c) for c in range(chunk)]
+        for e in range(local):
+            inside = slice(e * capacity, (e + 1) * capacity)
+            data = jnp.concatenate([rows_ref[s, inside, :] for s in at], axis=0)
+            gate = dot(data, switch_ref[e])
+            units = (gate / (1.0 + jnp.exp(-gate)) * dot(data, expand_ref[e])).astype(BF16)
+            value = dot(units, contract_ref[e]).astype(BF16)
+            for c in range(chunk):
+                y_ref[at[c], inside, :] = value[c * capacity : (c + 1) * capacity]
+        for s in at:
+            for g in others():
+                sib_copy(s, g).start()
+            sib_copy(s, group).start()
+
+    def meet(s):
         for g in others():
-            sib_copy(s, g).start()
-        sib_copy(s, group).start()
+            sib_copy(s, g).wait_recv()
+            pair[s, g] = (
+                y_ref[s, :, span(g * 2 + core, cols)].astype(F32) + from_sib[s, g].astype(F32)
+            ).astype(BF16)
+            peer_copy(s, g).start()
+        sib_copy(s, group).wait_recv()
+
+    def total_up(s):
+        total = y_ref[s, :, mine].astype(F32) + from_sib[s, group].astype(F32)
+        for g in others():
+            copy_to(
+                from_peer.at[s, g],
+                from_peer.at[s, g],
+                s_peer.at[s, g],
+                r_peer.at[s, g],
+                {"tp": g * 2 + core},
+            ).wait_recv()
+            total = total + from_peer[s, g].astype(F32)
+
+        @pl.when(s != sp)
+        def _():
+            summed[s] = total.astype(BF16)
+            back_copy(s).start()
+
+        @pl.when(s == sp)
+        def _():
+            back[s] = total.astype(BF16)
+
+    def step(i, carry):
+        @pl.when(i < chunks)
+        def _():
+            expert(i)
+
+        @pl.when((i >= 1) & (i <= chunks))
+        def _():
+            for c in range(chunk):
+                meet(order((i - 1) * chunk + c))
+
+        @pl.when(i >= 2)
+        def _():
+            for c in range(chunk):
+                total_up(order((i - 2) * chunk + c))
+
         return carry
 
-    lax.fori_loop(0, sp_count, open_up, 0)
-    lag = 2
-
-    def step(d, carry):
-        @pl.when(d < sp_count)
-        def _():
-            s = order(d)
-            for g in others():
-                sib_copy(s, g).wait_recv()
-                pair[s, g] = (
-                    y_ref[s, :, span(g * 2 + core, cols)].astype(F32) + from_sib[s, g].astype(F32)
-                ).astype(BF16)
-                peer_copy(s, g).start()
-            sib_copy(s, group).wait_recv()
-
-        @pl.when(d >= lag)
-        def _():
-            s = order(d - lag)
-            total = y_ref[s, :, mine].astype(F32) + from_sib[s, group].astype(F32)
-            for g in others():
-                copy_to(
-                    from_peer.at[s, g],
-                    from_peer.at[s, g],
-                    s_peer.at[s, g],
-                    r_peer.at[s, g],
-                    {"tp": g * 2 + core},
-                ).wait_recv()
-                total = total + from_peer[s, g].astype(F32)
-
-            @pl.when(s != sp)
-            def _():
-                summed[s] = total.astype(BF16)
-                back_copy(s).start()
-
-            @pl.when(s == sp)
-            def _():
-                back[s] = total.astype(BF16)
-
-        return carry
-
-    lax.fori_loop(0, sp_count + lag, step, 0)
+    lax.fori_loop(0, chunks + 2, step, 0)
     slots = slot_ref[...]
     weights = weight_ref[...]
     places = lax.broadcasted_iota(jnp.int32, (rows, sp_count * per), 1)
@@ -708,24 +736,13 @@
         * specialist_chance_within_cluster
         / jnp.sum(specialist_chance_within_cluster, axis=1, keepdims=True)
     )
-    grouped = rows_in.reshape(sp_count, local_experts, capacity, model_width)
-    gate_act = jnp.einsum(
-        "secd,edf->secf", grouped, specialist_switch_matrix, preferred_element_type=jnp.float32
-    )
-    upward = jnp.einsum(
-        "secd,edf->secf", grouped, specialist_expansion_matrix, preferred_element_type=jnp.float32
-    )
-    hidden = (jax.nn.silu(gate_act) * upward).astype(jnp.bfloat16)
-    partial_value = jnp.einsum(
-        "secf,efd->secd", hidden, specialist_contraction_matrix, preferred_element_type=jnp.float32
-    )
-    partial_value = partial_value.astype(jnp.bfloat16).reshape(rows_in.shape)
     return pl.pallas_call(
         functools.partial(return_kernel, sp_count, tp_count),
         out_shape=jax.ShapeDtypeStruct((tok_rows, model_width), BF16),
-        in_specs=[vmem] * 4,
+        in_specs=[vmem] * 7,
         out_specs=vmem,
         scratch_shapes=[
+            pltpu.VMEM((sp_count, per, model_width), BF16),
             pltpu.VMEM((sp_count, groups, per, cols), BF16),
             pltpu.VMEM((sp_count, groups, per, cols), BF16),
             pltpu.VMEM((sp_count, groups, per, cols), BF16),
@@ -744,7 +761,15 @@
         compiler_params=pltpu.CompilerParams(
             collective_id=3, has_side_effects=True, vmem_limit_bytes=50 * 1024 * 1024
         ),
-    )(partial_value, hidden_cols, slots, route_weight)
+    )(
+        rows_in,
+        specialist_switch_matrix,
+        specialist_expansion_matrix,
+        specialist_contraction_matrix,
+        hidden_cols,
+        slots,
+        route_weight,
+    )
 
 
 def solution(mesh):

time: 202 us -> 184 us (0.911)
  matrix products: 13.9 us -> 0 us
  Pallas kernels: 171 us -> 166 us
    dot_general x2 -> x0, matrix products: 13.9 us -> none  [the longest x1 10.2 us: body(): jnp.einsum('secf,efd->secd', hidden, specialist_contraction_matrix, prefe...]
    pallas_call x1, Pallas kernels: 45.7 us -> 37.4 us  [mixer_branch(): pl.pallas_call(functools.partial(mixer_kernel, head_dim, segment), grid=(...]
    pallas_call x1, Pallas kernels: 48.3 us -> 51.8 us  [body(): pl.pallas_call(functools.partial(return_kernel, sp_count, tp_count), out_...]
    unnamed x41 -> x39, local copies, waits for them, and re-layouts: 13 us -> 13.9 us
where the time goes in v3:
time: 184 us; the launch traced here: 181 us
  Pallas kernels  166 us (90%)
  local copies, waits for them, and re-layouts  14.1 us (8%)
    pallas_call x1, Pallas kernels, body(): pl.pallas_call(functools.partial(route_kernel, sp_count, tp_count, expert...  52.2 us
    pallas_call x1, Pallas kernels, body(): pl.pallas_call(functools.partial(return_kernel, sp_count, tp_count), out_...  51.8 us
    pallas_call x1, Pallas kernels, mixer_branch(): pl.pallas_call(functools.partial(mixer_kernel, head_dim, segment), grid=(...  37.4 us
    pallas_call x1, Pallas kernels, mixer_branch(): pl.pallas_call(functools.partial(exchange_kernel, count, per, workers), o...  17.8 us
    unnamed x39, local copies, waits for them, and re-layouts  13.9 us
    pallas_call x1, Pallas kernels, mixer_branch(): pl.pallas_call(functools.partial(finish_kernel, head_dim), grid=(model_wi...  7 us

profile of v3, /device:TPU:0, one launch (start us, length us, event | category | flops | bytes accessed | tf_op | source)
XLA Modules:
  0.0 180.7 jit_solution(16409916636534032124)
XLA Ops:
  0.0 0.8 copy.21.b_ref
  0.8 0.0 copy-start.7
  0.8 1.0 copy-done.7
  1.9 0.0 copy-start.9
  1.9 0.9 copy-done.9
  2.8 0.0 copy-start.10
  2.8 0.9 copy-done.10
  3.8 0.0 copy-start.11
  3.8 0.9 copy-done.11
  4.7 0.0 copy-start.12
  4.7 0.9 copy-done.12
  5.7 37.4 %shard_map.154 = (f32[256,512]{1,0:T(8,128)S(1)}, bf16[256,512]{1,0:T(8,128)(2,1)S(1)}, bf16[8,64,128]{2,1,0:T(8,128)(2,1)S(1)}) custom-call(bf16[256,512]{1,0:T(8,128)(2,1)S(1)} %copy-done.9, bf16[256,512]{1,0:T(8,128)(2,1)S(1)} %copy-done.10, bf16[256,512]{1,0:T(8,128)(2,1)S(1)} %copy-done.11, bf16[256,512]{1,0:T(8,128)(2,1)S(1)} %copy-done.12, ...), custom_call_target="tpu_custom_call" | custom-call | tf_op jit(solution)/shard_map/pallas_call | solution.py:248
  43.0 0.0 copy-start.6
  43.0 0.8 copy-done.6
  43.8 0.0 copy-start.8
  43.8 0.7 copy-done.8
  44.5 0.0 copy-start.13
  44.5 0.7 copy-done.13
  45.2 17.8 %shard_map.155.st_ref = bf16[8,64,128]{2,1,0:T(8,128)(2,1)} custom-call(bf16[8,64,128]{2,1,0:T(8,128)(2,1)} %copy-done.13), custom_call_target="tpu_custom_call" | custom-call | tf_op jit(solution)/shard_map/pallas_call | solution.py:263
  63.1 0.0 copy-start.15
  63.1 0.0 copy-start.3
  63.1 0.0 copy-start.14
  63.1 0.0 copy-start.2
  63.1 7.0 %shard_map.156.part_ref = bf16[256,2048]{1,0:T(8,128)(2,1)} custom-call(f32[256,512]{1,0:T(8,128)} %copy-done.6, bf16[256,512]{1,0:T(8,128)(2,1)} %copy-done.8, bf16[8,64,128]{2,1,0:T(8,128)(2,1)} %shard_map.155.st_ref, f32[1,512]{1,0:T(1,128)} %bitcast.3, bf16[512,2048]{1,0:T(8,128)(2,1)} %w_ref.1), custom_call_target="tpu_custom_call" | custom-call | tf_op jit(solution)/shard_map/pallas_call | solution.py:281
  70.1 0.0 copy-done.15
  70.1 0.0 copy-start.16
  70.1 0.0 copy-start.17
  70.1 0.1 copy.22.ids_ref
  70.3 0.0 copy-done.3
  70.3 0.0 copy-done.14
  70.3 0.0 copy-start.1
  70.3 1.2 copy-done.1
  71.5 52.2 %shard_map.157 = (f32[256,512]{1,0:T(8,128)S(1)}, s32[256,2]{1,0:T(8,128)S(1)}, bf16[8,128,2048]{2,1,0:T(8,128)(2,1)S(1)}) custom-call(bf16[256,2048]{1,0:T(8,128)(2,1)S(1)} %copy-done.1, bf16[256,2048]{1,0:T(8,128)(2,1)S(1)} %copy-done.3, f32[1,2048]{1,0:T(1,128)S(1)} %bitcast.2, s32[256,2]{1,0:T(8,128)S(1)} %copy.22.ids_ref), custom_call_target="tpu_custom_call" | custom-call | tf_op jit(solution)/shard_map/pallas_call | solution.py:702
  123.8 0.0 copy-start
  123.8 1.9 %copy-done = bf16[8,128,2048]{2,1,0:T(8,128)(2,1)} copy-done((bf16[8,128,2048]{2,1,0:T(8,128)(2,1)}, bf16[8,128,2048]{2,1,0:T(8,128)(2,1)S(1)}, u32[]{:S(2)}) %copy-start) | copy-done | bytes 4194328
  125.7 0.0 copy-start.4
  125.7 0.8 copy-done.4
  126.5 0.0 copy-done.16
  126.5 0.0 copy-done.17
  126.5 0.1 copy.23
  126.7 0.1 broadcast_divide_fusion.weight_ref
  126.8 0.0 copy-done.2
  126.8 0.0 copy-start.5
  126.8 1.0 copy-done.5
  127.9 51.8 %shard_map.158 = bf16[256,2048]{1,0:T(8,128)(2,1)S(1)} custom-call(bf16[8,128,2048]{2,1,0:T(8,128)(2,1)} %copy-done, bf16[1,2048,512]{2,1,0:T(8,128)(2,1)S(1)} %copy-done.2, bf16[1,2048,512]{2,1,0:T(8,128)(2,1)} %expand_ref.1, bf16[1,512,2048]{2,1,0:T(8,128)(2,1)} %contract_ref.1, f32[256,512]{1,0:T(8,128)S(1)} %copy-done.5, ...), custom_call_target="tpu_custom_call" | custom-call | tf_op jit(solution)/shard_map/pallas_call | solution.py:739
  179.7 1.0 copy.26
  (1 shorter events, 0.0 us)
Async XLA Ops:
  0.8 1.0 copy-start.7
  1.9 0.9 copy-start.9
  2.8 0.9 copy-start.10
  3.8 0.9 copy-start.11
  4.7 0.9 copy-start.12
  43.0 0.8 copy-start.6
  43.8 0.7 copy-start.8
  44.5 0.7 copy-start.13
  63.1 7.0 %copy-start.15 = (s32[256,2]{0,1:T(2,128)S(1)}, s32[256,2]{0,1:T(2,128)}, u32[]{:S(2)}) copy-start(s32[256,2]{0,1:T(2,128)} %param.28) | copy-start | bytes 6148
  63.1 7.2 %copy-start.3 = (bf16[256,2048]{1,0:T(8,128)(2,1)S(1)}, bf16[256,2048]{1,0:T(8,128)(2,1)}, u32[]{:S(2)}) copy-start(bf16[256,2048]{1,0:T(8,128)(2,1)} %skip_ref.1) | copy-start | bytes 3145732
  63.1 7.2 %copy-start.14 = (f32[2048]{0:T(1024)S(1)}, f32[2048]{0:T(1024)}, u32[]{:S(2)}) copy-start(f32[2048]{0:T(1024)} %param.25) | copy-start | bytes 24580
  63.1 63.7 %copy-start.2 = (bf16[1,2048,512]{2,1,0:T(8,128)(2,1)S(1)}, bf16[1,2048,512]{2,1,0:T(8,128)(2,1)}, u32[]{:S(2)}) copy-start(bf16[1,2048,512]{2,1,0:T(8,128)(2,1)} %switch_ref.1) | copy-start | bytes 6291460
  70.1 56.4 %copy-start.16 = (f32[256,2]{0,1:T(2,128)S(1)}, f32[256,2]{0,1:T(2,128)}, u32[]{:S(2)}) copy-start(f32[256,2]{0,1:T(2,128)} %param.27) | copy-start | bytes 6148
  70.1 56.4 %copy-start.17 = (f32[256]{0:T(256)S(1)}, f32[256]{0:T(256)}, u32[]{:S(2)}) copy-start(f32[256]{0:T(256)} %param.26) | copy-start | bytes 3076
  70.3 1.2 copy-start.1
  123.8 2.0 %copy-start = (bf16[8,128,2048]{2,1,0:T(8,128)(2,1)}, bf16[8,128,2048]{2,1,0:T(8,128)(2,1)S(1)}, u32[]{:S(2)}) copy-start(bf16[8,128,2048]{2,1,0:T(8,128)(2,1)S(1)} %get-tuple-element.14.rows_ref) | copy-start | bytes 12582916
  125.7 0.8 copy-start.4
  126.8 1.0 copy-start.5

commit v4 on v3

--- a/solution.py
+++ b/solution.py
@@ -255,7 +255,7 @@
             jax.ShapeDtypeStruct((rows, channels), BF16),
             jax.ShapeDtypeStruct((heads, head_dim, width), BF16),
         ],
-        compiler_params=pltpu.CompilerParams(vmem_limit_bytes=50 * 1024 * 1024),
+        compiler_params=pltpu.CompilerParams(vmem_limit_bytes=61 * 1024 * 1024),
     )(query, key, value, step, forget, bias)
     per = max(1, heads // count)
     workers = heads // per

time: 184 us -> 179 us (0.973)
  local copies, waits for them, and re-layouts: 14.1 us -> 7.75 us
  Pallas kernels: 166 us -> 168 us
    unnamed x39 -> x23, local copies, waits for them, and re-layouts: 13.9 us -> 7.61 us
where the time goes in v4:
time: 179 us; the launch traced here: 176 us
  Pallas kernels  168 us (94%)
  local copies, waits for them, and re-layouts  7.75 us (4%)
    pallas_call x1, Pallas kernels, body(): pl.pallas_call(functools.partial(route_kernel, sp_count, tp_count, expert...  52.2 us
    pallas_call x1, Pallas kernels, body(): pl.pallas_call(functools.partial(return_kernel, sp_count, tp_count), out_...  51.9 us
    pallas_call x1, Pallas kernels, mixer_branch(): pl.pallas_call(functools.partial(mixer_kernel, head_dim, segment), grid=(...  39 us
    pallas_call x1, Pallas kernels, mixer_branch(): pl.pallas_call(functools.partial(exchange_kernel, count, per, workers), o...  17.8 us
    unnamed x23, local copies, waits for them, and re-layouts  7.61 us
    pallas_call x1, Pallas kernels, mixer_branch(): pl.pallas_call(functools.partial(finish_kernel, head_dim), grid=(model_wi...  7 us

profile of v4, /device:TPU:0, one launch (start us, length us, event | category | flops | bytes accessed | tf_op | source)
XLA Modules:
  0.0 175.9 jit_solution(18038447970227625506)
XLA Ops:
  0.0 1.5 copy.21.b_ref
  1.5 39.0 %shard_map.154 = (f32[256,512]{1,0:T(8,128)}, bf16[256,512]{1,0:T(8,128)(2,1)}, bf16[8,64,128]{2,1,0:T(8,128)(2,1)}) custom-call(bf16[256,512]{1,0:T(8,128)(2,1)} %q_ref.1, bf16[256,512]{1,0:T(8,128)(2,1)} %k_ref.1, bf16[256,512]{1,0:T(8,128)(2,1)} %v_ref.1, bf16[256,512]{1,0:T(8,128)(2,1)} %a_ref.1, f32[256,512]{1,0:T(8,128)} %f_ref.1, f32[256,8]{1,0:T(8,128)} %copy.21.b_ref), custom_call_target="tpu_custom_call" | custom-call | tf_op jit(solution)/shard_map/pallas_call | solution.py:248
  40.5 17.8 %shard_map.155.st_ref = bf16[8,64,128]{2,1,0:T(8,128)(2,1)} custom-call(bf16[8,64,128]{2,1,0:T(8,128)(2,1)} %get-tuple-element.13.ka_ref), custom_call_target="tpu_custom_call" | custom-call | tf_op jit(solution)/shard_map/pallas_call | solution.py:263
  58.3 0.0 copy-start.7
  58.3 0.0 copy-start.3
  58.3 0.0 copy-start.6
  58.3 0.0 copy-start.2
  58.4 7.0 %shard_map.156.part_ref = bf16[256,2048]{1,0:T(8,128)(2,1)} custom-call(f32[256,512]{1,0:T(8,128)} %get-tuple-element.11.out_ref, bf16[256,512]{1,0:T(8,128)(2,1)} %get-tuple-element.12.map_ref, bf16[8,64,128]{2,1,0:T(8,128)(2,1)} %shard_map.155.st_ref, f32[1,512]{1,0:T(1,128)} %bitcast.3, bf16[512,2048]{1,0:T(8,128)(2,1)} %w_ref.1), custom_call_target="tpu_custom_call" | custom-call | tf_op jit(solution)/shard_map/pallas_call | solution.py:281
  65.4 0.0 copy-done.7
  65.4 0.0 copy-start.8
  65.4 0.0 copy-start.9
  65.4 0.1 copy.22.ids_ref
  65.5 0.0 copy-done.3
  65.5 0.0 copy-done.6
  65.5 0.0 copy-start.1
  65.5 1.2 copy-done.1
  66.8 52.2 %shard_map.157 = (f32[256,512]{1,0:T(8,128)S(1)}, s32[256,2]{1,0:T(8,128)S(1)}, bf16[8,128,2048]{2,1,0:T(8,128)(2,1)S(1)}) custom-call(bf16[256,2048]{1,0:T(8,128)(2,1)S(1)} %copy-done.1, bf16[256,2048]{1,0:T(8,128)(2,1)S(1)} %copy-done.3, f32[1,2048]{1,0:T(1,128)S(1)} %bitcast.2, s32[256,2]{1,0:T(8,128)S(1)} %copy.22.ids_ref), custom_call_target="tpu_custom_call" | custom-call | tf_op jit(solution)/shard_map/pallas_call | solution.py:702
  119.0 0.0 copy-start
  119.0 1.9 %copy-done = bf16[8,128,2048]{2,1,0:T(8,128)(2,1)} copy-done((bf16[8,128,2048]{2,1,0:T(8,128)(2,1)}, bf16[8,128,2048]{2,1,0:T(8,128)(2,1)S(1)}, u32[]{:S(2)}) %copy-start) | copy-done | bytes 4194328
  121.0 0.0 copy-start.4
  121.0 0.8 copy-done.4
  121.8 0.0 copy-done.8
  121.8 0.0 copy-done.9
  121.8 0.1 copy.23
  121.9 0.1 broadcast_divide_fusion.weight_ref
  122.0 0.0 copy-done.2
  122.0 0.0 copy-start.5
  122.1 1.0 copy-done.5
  123.1 51.9 %shard_map.158 = bf16[256,2048]{1,0:T(8,128)(2,1)S(1)} custom-call(bf16[8,128,2048]{2,1,0:T(8,128)(2,1)} %copy-done, bf16[1,2048,512]{2,1,0:T(8,128)(2,1)S(1)} %copy-done.2, bf16[1,2048,512]{2,1,0:T(8,128)(2,1)} %expand_ref.1, bf16[1,512,2048]{2,1,0:T(8,128)(2,1)} %contract_ref.1, f32[256,512]{1,0:T(8,128)S(1)} %copy-done.5, ...), custom_call_target="tpu_custom_call" | custom-call | tf_op jit(solution)/shard_map/pallas_call | solution.py:739
  175.0 1.0 copy.26
  (1 shorter events, 0.0 us)
Async XLA Ops:
  58.3 7.0 %copy-start.7 = (s32[256,2]{0,1:T(2,128)S(1)}, s32[256,2]{0,1:T(2,128)}, u32[]{:S(2)}) copy-start(s32[256,2]{0,1:T(2,128)} %param.28) | copy-start | bytes 6148
  58.3 7.2 %copy-start.3 = (bf16[256,2048]{1,0:T(8,128)(2,1)S(1)}, bf16[256,2048]{1,0:T(8,128)(2,1)}, u32[]{:S(2)}) copy-start(bf16[256,2048]{1,0:T(8,128)(2,1)} %skip_ref.1) | copy-start | bytes 3145732
  58.3 7.2 %copy-start.6 = (f32[2048]{0:T(1024)S(1)}, f32[2048]{0:T(1024)}, u32[]{:S(2)}) copy-start(f32[2048]{0:T(1024)} %param.25) | copy-start | bytes 24580
  58.3 63.7 %copy-start.2 = (bf16[1,2048,512]{2,1,0:T(8,128)(2,1)S(1)}, bf16[1,2048,512]{2,1,0:T(8,128)(2,1)}, u32[]{:S(2)}) copy-start(bf16[1,2048,512]{2,1,0:T(8,128)(2,1)} %switch_ref.1) | copy-start | bytes 6291460
  65.4 56.4 %copy-start.8 = (f32[256,2]{0,1:T(2,128)S(1)}, f32[256,2]{0,1:T(2,128)}, u32[]{:S(2)}) copy-start(f32[256,2]{0,1:T(2,128)} %param.27) | copy-start | bytes 6148
  65.4 56.4 %copy-start.9 = (f32[256]{0:T(256)S(1)}, f32[256]{0:T(256)}, u32[]{:S(2)}) copy-start(f32[256]{0:T(256)} %param.26) | copy-start | bytes 3076
  65.5 1.2 copy-start.1
  119.0 1.9 %copy-start = (bf16[8,128,2048]{2,1,0:T(8,128)(2,1)}, bf16[8,128,2048]{2,1,0:T(8,128)(2,1)S(1)}, u32[]{:S(2)}) copy-start(bf16[8,128,2048]{2,1,0:T(8,128)(2,1)S(1)} %get-tuple-element.14.rows_ref) | copy-start | bytes 12582916
  121.0 0.8 copy-start.4
  122.0 1.0 copy-start.5
